TPU v7x, 32 devices: a whole 2x2x4 slice. The times are simulated.
32 devices in a mesh: grp: 2 (over y), fs: 4 (over z), tp: 4 (over x, core).
Axes of the slice: x: 2, y: 2, z: 4, core: 2. Of those that a mesh axis runs over, the one named last changes fastest.
Arguments:
- tokens: bfloat16 [3072, 2048], P(('grp', 'fs'), 'tp'), parts along dimension 0, may hold values from -6 to 6
- mix_gain: float32 [2048], replicated, may hold values from 0.1 to 1.9
- w_signal: bfloat16 [2048, 1024], P('fs', 'tp'), may hold values from -0.125 to 0.125
- w_outer_gate: bfloat16 [2048, 1024], P('fs', 'tp'), may hold values from -0.125 to 0.125
- w_inner_gate: bfloat16 [2048, 1024], P('fs', 'tp'), may hold values from -0.125 to 0.125
- mix_taps: float32 [3, 1024], P(None, 'tp'), may hold values from -3 to 3
- w_mix_out: bfloat16 [1024, 2048], P('tp', 'fs'), may hold values from -0.1875 to 0.1875
- ffn_gain: float32 [2048], replicated, may hold values from 0.1 to 1.9
- w_gate: bfloat16 [2048, 5120], P('fs', 'tp'), may hold values from -0.125 to 0.125
- w_value: bfloat16 [2048, 5120], P('fs', 'tp'), may hold values from -0.125 to 0.125
- up_taps: float32 [2, 3, 5120], P(None, None, 'tp'), may hold values from -3 to 3
- up_bias: float32 [2, 5120], P(None, 'tp'), may hold values from -3 to 3
- w_down: bfloat16 [5120, 2048], P('tp', 'fs'), may hold values from -0.078125 to 0.078125
Outputs:
- layer_out: bfloat16 [3072, 2048], P(('grp', 'fs'), 'tp'), parts along dimension 0
There are 2 independent parts, one for each index of `grp`. A program takes and returns all parts, laid end to end along the dimension named above; an argument that names none is the same for every part. Nothing has to cross between parts.
All inputs are finite; a program needn't handle non-finite values.
Results may differ from a plain program's by a relative error of at most 0.022.
Values may be sent and summed in bfloat16 or wider, within the bound.
A program may use at most 64 MiB of HBM per device.

v0:
```python
import functools

import jax
import jax.numpy as jnp
from jax import lax
from jax.experimental import pallas as pl
from jax.experimental.pallas import tpu as pltpu
from jax.sharding import PartitionSpec as P

SEQS_DEV = 2


def conv_positions(values, taps):
    width = values.shape[1]
    blocks = values.reshape(SEQS_DEV, -1, width)
    length = blocks.shape[1]
    padded = jnp.pad(blocks, ((0, 0), (2, 0), (0, 0)))
    result = (
        padded[:, 0:length] * taps[0]
        + padded[:, 1 : length + 1] * taps[1]
        + padded[:, 2 : length + 2] * taps[2]
    )
    return result.reshape(-1, width)


def rms_norm(stream, gain):
    values = stream.astype(jnp.float32)
    scale = lax.rsqrt(jnp.mean(values * values, axis=-1, keepdims=True) + 1e-06)
    return (values * scale * gain).astype(jnp.bfloat16)


def on_device(
    tokens,
    mix_gain,
    w_signal,
    w_outer_gate,
    w_inner_gate,
    mix_taps,
    w_mix_out,
    ffn_gain,
    w_gate,
    w_value,
    up_taps,
    up_bias,
    w_down,
):
    whole = lax.all_gather(tokens, "tp", axis=1, tiled=True)
    normed = rms_norm(whole, mix_gain)
    pieces = (
        lax.all_gather(w_signal, "fs", axis=0, tiled=True),
        lax.all_gather(w_outer_gate, "fs", axis=0, tiled=True),
        lax.all_gather(w_inner_gate, "fs", axis=0, tiled=True),
    )
    columns = normed
    signal, outer, inner = tuple(
        (jnp.dot(columns, piece, preferred_element_type=jnp.float32) for piece in pieces)
    )
    signal = signal.astype(jnp.bfloat16).astype(jnp.float32)
    outer = outer.astype(jnp.bfloat16).astype(jnp.float32)
    inner = inner.astype(jnp.bfloat16).astype(jnp.float32)
    mixed = (outer * conv_positions(inner * signal, mix_taps)).astype(jnp.bfloat16)
    mix_terms = jnp.dot(
        mixed,
        lax.all_gather(w_mix_out, "fs", axis=1, tiled=True),
        preferred_element_type=jnp.float32,
    )
    mix_sum = lax.psum_scatter(
        mix_terms.astype(jnp.bfloat16), "tp", scatter_dimension=1, tiled=True
    ).astype(jnp.float32)
    resid = (tokens.astype(jnp.float32) + mix_sum).astype(jnp.bfloat16)
    whole_ffn = lax.all_gather(resid, "tp", axis=1, tiled=True)
    normed_ffn = rms_norm(whole_ffn, ffn_gain)
    pieces = (
        lax.all_gather(w_gate, "fs", axis=0, tiled=True),
        lax.all_gather(w_value, "fs", axis=0, tiled=True),
    )
    columns = normed_ffn
    gate = jnp.dot(columns, pieces[0], preferred_element_type=jnp.float32)
    value = jnp.dot(columns, pieces[1], preferred_element_type=jnp.float32)
    gate = gate.astype(jnp.bfloat16).astype(jnp.float32)
    value = value.astype(jnp.bfloat16).astype(jnp.float32)
    gate_conv = conv_positions(gate, up_taps[0]) + up_bias[0]
    value_conv = conv_positions(value, up_taps[1]) + up_bias[1]
    hidden = (jax.nn.silu(gate_conv) * value_conv).astype(jnp.bfloat16)
    ffn_terms = jnp.dot(
        hidden, lax.all_gather(w_down, "fs", axis=1, tiled=True), preferred_element_type=jnp.float32
    )
    ffn_sum = lax.psum_scatter(
        ffn_terms.astype(jnp.bfloat16), "tp", scatter_dimension=1, tiled=True
    ).astype(jnp.float32)
    return (resid.astype(jnp.float32) + ffn_sum).astype(jnp.bfloat16)


MESH = pl.DeviceIdType.MESH
UP, DOWN = 0, 1
LANES = 128


def shifted(values, by, length):
    rolled = pltpu.roll(values, by, 0)
    position = lax.rem(lax.broadcasted_iota(jnp.int32, values.shape, 0), length)
    return jnp.where(position < by, 0.0, rolled)


def conv_rows(values, taps, length):
    return (
        shifted(values, 2, length) * taps[0:1]
        + shifted(values, 1, length) * taps[1:2]
        + values * taps[2:3]
    )


def layer_kernel(
    n_fs,
    n_tp,
    tokens,
    mix_gain,
    w_signal,
    w_outer_gate,
    w_inner_gate,
    mix_taps,
    w_mix_out,
    ffn_gain,
    w_gate,
    w_value,
    up_taps,
    up_bias,
    w_down,
    out,
    mix_in,
    mix_out,
    ffn_in,
    ffn_out,
    tok,
    res,
    normed,
    hidden,
    part,
    got,
    part_ffn,
    got_core,
    sum_x,
    got_x,
    sum_z,
    got_z,
    z_send,
    z_recv,
    y_send,
    y_recv,
    load_sem,
    tp_send,
    tp_recv,
    all_send,
    all_recv,
    core_send,
    core_recv,
    x_send,
    x_recv,
    pair_send,
    pair_recv,
):
    g, j, k = lax.axis_index("grp"), lax.axis_index("fs"), lax.axis_index("tp")
    rows, own_cols = tokens.shape
    length = rows // SEQS_DEV
    shard, chans = w_signal.shape
    half = shard // 2
    hidden_half = w_gate.shape[1] // 2
    n_in, n_out = hidden_half // LANES, shard // LANES
    n_x = n_tp // 2
    x, c = k // 2, lax.rem(k, 2)
    core = k + 1 - 2 * c
    p = lax.rem(j, 2)
    pair = j + 1 - 2 * p
    mine = pl.ds(pl.multiple_of(p * rows, rows), rows)
    theirs = pl.ds(pl.multiple_of((1 - p) * rows, rows), rows)

    mix = ("mix", 0)
    order = [mix, *(("in", t) for t in range(n_in)), *(("out", u) for u in range(n_out))]

    def chunks(stage):
        return (None,) if stage[0] == "mix" else (0, 1)

    def top(q):
        return n_fs - 1 if q is None or (n_fs - 1) % 2 == q else n_fs - 2

    def bottom(q):
        return 0 if q is None else q

    def views(stage, q, source, side):
        kind, i = stage
        at_rows = pl.ds(pl.multiple_of((source * 2 + side) * half, half), half)
        tall = (chans if kind == "mix" else hidden_half) // 2
        at_chans = pl.ds(pl.multiple_of(side * tall, tall), tall)
        if kind == "mix":
            return mix_in.at[:, at_rows, :], mix_out.at[source, at_chans, :]
        if kind == "in":
            return (ffn_in.at[i, q, at_rows, :],)
        lanes = pl.ds(pl.multiple_of(source * LANES, LANES), LANES)
        return (ffn_out.at[i, q, at_chans, lanes],)

    def slot(stage, q, i):
        kind, at = stage
        if kind == "mix":
            return i
        return 2 + 2 * (at if kind == "in" else at + n_in) + q

    def z_copies(s, q, source, way):
        return [
            pltpu.make_async_remote_copy(
                src_ref=view,
                dst_ref=view,
                send_sem=z_send.at[way, slot(s, q, i), source],
                recv_sem=z_recv.at[slot(s, q, i), source],
                device_id={"fs": j + 1 if way == UP else j - 1},
                device_id_type=MESH,
            )
            for i, view in enumerate(views(s, q, source, g))
        ]

    def y_copies(s, q, source, side):
        return [
            pltpu.make_async_remote_copy(
                src_ref=view,
                dst_ref=view,
                send_sem=y_send.at[slot(s, q, i), source],
                recv_sem=y_recv.at[slot(s, q, i), source],
                device_id={"grp": 1 - g},
                device_id_type=MESH,
            )
            for i, view in enumerate(views(s, q, source, side))
        ]

    def start(copies):
        for copy in copies:
            copy.start()

    def wait_recv(copies):
        for copy in copies:
            copy.wait_recv()

    def wait_send(copies):
        for copy in copies:
            copy.wait_send()

    def goes_on(q, way):
        return j + 1 <= top(q) if way == UP else j - 1 >= bottom(q)

    def comes(q, source, way):
        if way == UP:
            return (source >= 0) & (j <= top(q))
        return (source < n_fs) & (j >= bottom(q))

    def own(s, way):
        for q in chunks(s):

            @pl.when(goes_on(q, way))
            def _():
                start(z_copies(s, q, j, way))

    def relay(s):
        at = order.index(s)
        following = order[at + 2 : at + 3] if at else order[1:3]
        for d in range(1, n_fs):
            for q in chunks(s):
                for way, source in ((UP, j - d), (DOWN, j + d)):

                    @pl.when(comes(q, source, way))
                    def _():
                        wait_recv(z_copies(s, q, source, way))

                        @pl.when(goes_on(q, way))
                        def _():
                            start(z_copies(s, q, source, way))

                        if q is None:
                            start(y_copies(s, q, source, g))
                        else:

                            @pl.when(p == q)
                            def _():
                                start(y_copies(s, q, source, g))

            if following:

                @pl.when((j == d) & (j + 1 < n_fs))
                def _():
                    for later in following:
                        own(later, UP)

                @pl.when((n_fs - 1 - j == d) & (j >= 1))
                def _():
                    for later in following:
                        own(later, DOWN)

    def arrived(s):
        q = None if s[0] == "mix" else p
        for d in range(1, n_fs):
            wait_recv(y_copies(s, q, lax.rem(j + d, n_fs), 1 - g))

    def to_tp(src, dst, send_sem, recv_sem, to):
        return pltpu.make_async_remote_copy(
            src_ref=src,
            dst_ref=dst,
            send_sem=send_sem,
            recv_sem=recv_sem,
            device_id={"tp": to},
            device_id_type=MESH,
        )

    def tok_copy(d, source):
        return to_tp(
            tok.at[source], tok.at[source], tp_send.at[0, d], tp_recv.at[0, d], lax.rem(k + d, n_tp)
        )

    def mix_copy(d):
        to = lax.rem(k + d, n_tp)
        return to_tp(part.at[to], got.at[d], tp_send.at[1, d], tp_recv.at[1, d], to)

    def all_copies(o, at, kind):
        copies = []
        for dx in range(n_x):
            there = lax.rem(x + dx, n_x)
            if kind == "over":
                if dx:
                    view = res.at[k, at]
                    copies.append(
                        to_tp(
                            view,
                            view,
                            all_send.at[o, 0, dx],
                            all_recv.at[o, 0, dx],
                            there * 2 + c,
                        )
                    )
            else:
                back = lax.rem(x + n_x - dx, n_x) * 2
                seen = back + c if kind == "pass" else back + 1 - c
                view = res.at[seen, at]
                copies.append(
                    to_tp(view, view, all_send.at[o, 1, dx], all_recv.at[o, 1, dx], core)
                )
        return copies

    def all_begin(o, at):
        start(all_copies(o, at, "over"))
        all_copies(o, at, "pass")[0].start()

    def all_middle(o, at):
        passed = all_copies(o, at, "pass")
        for dx in range(1, n_x):
            view = res.at[lax.rem(x + n_x - dx, n_x) * 2 + c, at]
            to_tp(
                view, view, all_send.at[o, 0, dx], all_recv.at[o, 0, dx], core
            ).wait_recv()
            passed[dx].start()

    def all_end(o, at):
        wait_recv(all_copies(o, at, "take"))

    def to_pair(i, src, dst):
        return pltpu.make_async_remote_copy(
            src_ref=src,
            dst_ref=dst,
            send_sem=pair_send.at[i],
            recv_sem=pair_recv.at[i],
            device_id={"fs": pair},
            device_id_type=MESH,
        )

    barrier = pltpu.get_barrier_semaphore()
    for peer in (lax.rem(j + 1, n_fs), lax.rem(j + n_fs - 1, n_fs)):
        pl.semaphore_signal(barrier, inc=1, device_id={"fs": peer}, device_id_type=MESH)
    pl.semaphore_signal(barrier, inc=1, device_id={"grp": 1 - g}, device_id_type=MESH)
    for d in range(1, n_tp):
        pl.semaphore_signal(
            barrier, inc=1, device_id={"tp": lax.rem(k + d, n_tp)}, device_id_type=MESH
        )

    at_rows = pl.ds(pl.multiple_of(j * shard, shard), shard)
    loads = [
        pltpu.make_async_copy(ref, mix_in.at[i, at_rows, :], load_sem.at[i])
        for i, ref in enumerate((w_signal, w_outer_gate, w_inner_gate))
    ]
    loads.append(pltpu.make_async_copy(w_mix_out, mix_out.at[j], load_sem.at[3]))
    loads.append(pltpu.make_async_copy(tokens, tok.at[k], load_sem.at[4]))
    for q in (0, 1):
        for t in range(n_in):
            at = pl.ds(q * hidden_half + t * LANES, LANES)
            for i, ref in enumerate((w_gate, w_value)):
                dst = ffn_in.at[t, q, at_rows, pl.ds(i * LANES, LANES)]
                loads.append(pltpu.make_async_copy(ref.at[:, at], dst, load_sem.at[len(loads)]))
        for u in range(n_out):
            src = w_down.at[pl.ds(q * hidden_half, hidden_half), pl.ds(u * LANES, LANES)]
            lanes = pl.ds(pl.multiple_of(j * LANES, LANES), LANES)
            dst = ffn_out.at[u, q, :, lanes]
            loads.append(pltpu.make_async_copy(src, dst, load_sem.at[len(loads)]))
    start(loads)
    for copy in loads[:5]:
        copy.wait()
    pl.semaphore_wait(barrier, 3 + n_tp - 1)

    own(mix, UP)
    own(mix, DOWN)
    for d in range(1, n_tp):
        tok_copy(d, k).start()
    for copy in loads[5:]:
        copy.wait()

    @pl.when(j == 0)
    def _():
        for s in order[1:]:
            own(s, UP)

    @pl.when(j == n_fs - 1)
    def _():
        for s in order[1:]:
            own(s, DOWN)

    def norm(buffer, at, gain):
        squares = jnp.zeros((rows, 1), jnp.float32)
        for b in range(n_tp):
            values = buffer[b, at, :].astype(jnp.float32)
            squares = squares + jnp.sum(values * values, axis=-1, keepdims=True)
        scale = lax.rsqrt(squares / (n_tp * own_cols) + 1e-06)
        for b in range(n_tp):
            cut = slice(b * own_cols, (b + 1) * own_cols)
            values = buffer[b, at, :].astype(jnp.float32)
            normed[at, cut] = (values * scale * gain[:, cut]).astype(jnp.bfloat16)

    first = pl.ds(0, rows)
    for d in range(1, n_tp):
        tok_copy(d, lax.rem(k + n_tp - d, n_tp)).wait_recv()
    norm(tok, first, mix_gain)

    relay(mix)
    relay(order[1])
    arrived(mix)

    def project(weight):
        product = jnp.dot(normed[first, :], weight, preferred_element_type=jnp.float32)
        return product.astype(jnp.bfloat16).astype(jnp.float32)

    gated = project(mix_in[2]) * project(mix_in[0])
    conv = conv_rows(gated, mix_taps[...], length)
    mixed = (project(mix_in[1]) * conv).astype(jnp.bfloat16)
    for b in range(n_fs):
        part[b] = jnp.dot(mixed, mix_out[b], preferred_element_type=jnp.float32).astype(jnp.bfloat16)
    for d in range(1, n_tp):
        mix_copy(d).start()


    mixer = part[k].astype(jnp.float32)
    for d in range(1, n_tp):
        mix_copy(d).wait_recv()
        mixer = mixer + got[d].astype(jnp.float32)
    res[k, mine, :] = (tok[k].astype(jnp.float32) + mixer).astype(jnp.bfloat16)
    swap = to_pair(0, res.at[k, mine], res.at[k, mine])
    swapped = to_pair(0, res.at[k, theirs], res.at[k, theirs])
    swap.start()
    all_begin(0, mine)

    relay(order[2])
    all_middle(0, mine)
    swapped.wait_recv()
    all_begin(1, theirs)
    all_end(0, mine)
    norm(res, mine, ffn_gain)
    relay(order[3])
    all_middle(1, theirs)
    all_end(1, theirs)
    norm(res, theirs, ffn_gain)
    relay(order[4])

    def feed(t):
        arrived(("in", t))
        cut = pl.ds(pl.multiple_of(p * hidden_half + t * LANES, LANES), LANES)
        both = jnp.dot(normed[...], ffn_in[t, p], preferred_element_type=jnp.float32)
        both = both.astype(jnp.bfloat16).astype(jnp.float32)
        gate = conv_rows(both[:, :LANES], up_taps[0, :, cut], length) + up_bias[0:1, cut]
        value = conv_rows(both[:, LANES:], up_taps[1, :, cut], length) + up_bias[1:2, cut]
        units = (gate / (1.0 + jnp.exp(-gate)) * value).astype(jnp.bfloat16)
        hidden[:, pl.ds(pl.multiple_of(t * LANES, LANES), LANES)] = units

    beside = {0: 5, 1: 6, 3: 7}

    @pl.loop(0, n_in)
    def _(t):
        for at, index in beside.items():

            @pl.when(t == at)
            def _():
                relay(order[index])

        feed(t)

    def core_copy(u, dx):
        there = lax.rem(x + dx, n_x)
        return to_tp(
            part_ffn.at[u, :, there * 2 + 1 - c],
            got_core.at[u, :, there],
            core_send.at[u, dx],
            core_recv.at[u, dx],
            core,
        )

    def x_copy(u, dx):
        to = lax.rem(x + dx, n_x) * 2 + c
        return to_tp(sum_x.at[u, dx], got_x.at[u, dx], x_send.at[u, dx], x_recv.at[u, dx], to)

    def back(u):
        return to_pair(1 + u, sum_z.at[u], got_z.at[u])

    def chip_sum(u, o, dx):
        there = lax.rem(x + dx, n_x)
        mine_there = part_ffn[u, o, there * 2 + c].astype(jnp.float32)
        return mine_there + got_core[u, o, there].astype(jnp.float32)

    def place_sum(u, o):
        value = chip_sum(u, o, 0)
        for dx in range(1, n_x):
            value = value + got_x[u, dx, o].astype(jnp.float32)
        return value

    def down(u):
        arrived(("out", u))
        for o, at in enumerate((theirs, mine)):
            terms = jnp.dot(hidden[at, :], ffn_out[u, p], preferred_element_type=jnp.float32)
            for b in range(n_tp):
                part_ffn[u, o, b] = terms[:, b * LANES : (b + 1) * LANES].astype(jnp.bfloat16)
        for dx in (*range(1, n_x), 0):
            core_copy(u, dx).start()

    def over_x(u):
        for dx in range(1, n_x):
            core_copy(u, dx).wait_recv()
            for o in (0, 1):
                sum_x[u, dx, o] = chip_sum(u, o, dx).astype(jnp.bfloat16)
            x_copy(u, dx).start()

    def over_z(u):
        core_copy(u, 0).wait_recv()
        for dx in range(1, n_x):
            x_copy(u, dx).wait_recv()
        sum_z[u] = place_sum(u, 0).astype(jnp.bfloat16)
        back(u).start()

    for u in range(n_out):
        if 8 + u < len(order):
            relay(order[8 + u])
        down(u)
        if u >= 1:
            over_x(u - 1)
        if u >= 2:
            over_z(u - 2)
    over_x(n_out - 1)
    for u in range(max(n_out - 2, 0), n_out):
        over_z(u)
    for u in range(n_out):
        cut = slice(u * LANES, (u + 1) * LANES)
        value = res[k, mine, cut].astype(jnp.float32) + place_sum(u, 1)
        back(u).wait_recv()
        out[:, cut] = (value + got_z[u].astype(jnp.float32)).astype(jnp.bfloat16)

    for d in range(1, n_tp):
        tok_copy(d, k).wait_send()
        mix_copy(d).wait_send()
    for o, at in enumerate((mine, theirs)):
        wait_send(all_copies(o, at, "over"))
        wait_send(all_copies(o, at, "pass"))
    for u in range(n_out):
        for dx in range(n_x):
            core_copy(u, dx).wait_send()
        for dx in range(1, n_x):
            x_copy(u, dx).wait_send()
        back(u).wait_send()
    swap.wait_send()

    def drain(s):
        for q in chunks(s):
            for d in range(n_fs):
                for way, source in ((UP, j - d), (DOWN, j + d)):

                    @pl.when(comes(q, source, way) & goes_on(q, way))
                    def _():
                        wait_send(z_copies(s, q, source, way))

        q = None if s[0] == "mix" else p
        for d in range(1, n_fs):
            wait_send(y_copies(s, q, lax.rem(j + d, n_fs), g))

    drain(mix)

    @pl.loop(0, n_in)
    def _(t):
        drain(("in", t))

    @pl.loop(0, n_out)
    def _(u):
        drain(("out", u))


def fused(n_fs, n_tp, *args):
    tokens, w_signal, w_gate = args[0], args[2], args[8]
    rows, cols = tokens.shape
    shard, chans = w_signal.shape
    hidden = w_gate.shape[1] // 2
    n_in, n_out = hidden // LANES, shard // LANES
    width = n_fs * shard
    args = list(args)
    args[1], args[7] = args[1].reshape(1, -1), args[7].reshape(1, -1)
    in_vmem = {1, 5, 7, 10, 11}
    n_x = n_tp // 2
    copies = 2 + 2 * (n_in + n_out)
    dma = pltpu.SemaphoreType.DMA

    def held(*shape):
        return pltpu.VMEM(shape, jnp.bfloat16)

    return pl.pallas_call(
        functools.partial(layer_kernel, n_fs, n_tp),
        out_shape=jax.ShapeDtypeStruct((rows, cols), jnp.bfloat16),
        in_specs=[
            pl.BlockSpec(memory_space=pltpu.VMEM if i in in_vmem else pl.ANY)
            for i in range(len(args))
        ],
        out_specs=pl.BlockSpec(memory_space=pltpu.VMEM),
        scratch_shapes=[
            held(3, width, chans),
            held(n_fs, chans, shard),
            held(n_in, 2, width, 2 * LANES),
            held(n_out, 2, hidden, n_fs * LANES),
            held(n_tp, rows, cols),
            held(n_tp, 2 * rows, cols),
            held(2 * rows, width),
            held(2 * rows, hidden),
            held(n_tp, rows, cols),
            held(n_tp, rows, cols),
            held(n_out, 2, n_tp, rows, LANES),
            held(n_out, 2, n_x, rows, LANES),
            held(n_out, n_x, 2, rows, LANES),
            held(n_out, n_x, 2, rows, LANES),
            held(n_out, rows, LANES),
            held(n_out, rows, LANES),
            dma((2, copies, n_fs)),
            dma((copies, n_fs)),
            dma((copies, n_fs)),
            dma((copies, n_fs)),
            dma((5 + 4 * n_in + 2 * n_out,)),
            dma((2, n_tp)),
            dma((2, n_tp)),
            dma((2, 2, n_x)),
            dma((2, 2, n_x)),
            dma((n_out, n_x)),
            dma((n_out, n_x)),
            dma((n_out, n_x)),
            dma((n_out, n_x)),
            dma((1 + n_out,)),
            dma((1 + n_out,)),
        ],
        compiler_params=pltpu.CompilerParams(
            collective_id=0, has_side_effects=True, vmem_limit_bytes=62 * 1024 * 1024
        ),
    )(*args)


def solution(mesh):
    n_fs, n_tp = mesh.shape["fs"], mesh.shape["tp"]
    body = functools.partial(fused, n_fs, n_tp)
    if n_fs > 8 or n_fs != n_tp or n_fs % 2 or mesh.shape["grp"] != 2:
        body = on_device
    placed = (
        P(("grp", "fs"), "tp"),
        P(),
        P("fs", "tp"),
        P("fs", "tp"),
        P("fs", "tp"),
        P(None, "tp"),
        P("tp", "fs"),
        P(),
        P("fs", "tp"),
        P("fs", "tp"),
        P(None, None, "tp"),
        P(None, "tp"),
        P("tp", "fs"),
    )
    return jax.shard_map(
        body, mesh=mesh, in_specs=placed, out_specs=P(("grp", "fs"), "tp"), check_vma=False
    )
```

profile of v0, /device:TPU:0, one launch (start us, length us, event | category | flops | bytes accessed | tf_op | source)
XLA Modules:
  0.0 174.7 jit_solution(9463818296446509466)
XLA Ops:
  0.0 1.4 copy.14.up_taps
  1.4 171.5 %shard_map.127 = bf16[384,512]{1,0:T(8,128)(2,1)} custom-call(bf16[384,512]{1,0:T(8,128)(2,1)} %tokens.1, f32[1,2048]{1,0:T(1,128)} %bitcast.2, bf16[512,256]{1,0:T(8,128)(2,1)} %w_signal.1, bf16[512,256]{1,0:T(8,128)(2,1)} %w_outer_gate.1, bf16[512,256]{1,0:T(8,128)(2,1)} %w_inner_gate.1, f32[3,256]{1,0:T(4,128)} %mix_taps.1, bf16[256,512]{1,0:T(8,128)(2,1)} %w_mix_out.1, ...), custom_call_target="tpu_custom_call" | custom-call | tf_op jit(solution)/shard_map/pallas_call | solution.py:619
  172.9 1.8 %copy.16 = bf16[384,512]{1,0:T(8,128)(2,1)} copy(bf16[384,512]{1,0:T(8,128)(2,1)} %shard_map.127) | data formatting | bytes 786432
where the time goes:
time: 176 us; the launch traced here: 175 us
  Pallas kernels  172 us (98%)
  local copies, waits for them, and re-layouts  3.15 us (2%)
    pallas_call x1, Pallas kernels, fused(): pl.pallas_call(functools.partial(layer_kernel, n_fs, n_tp), out_shape=jax...  172 us

commit v1 on v0

v1 whole, which is shorter than its diff:
```python
import functools

import jax
import jax.numpy as jnp
from jax import lax
from jax.experimental import pallas as pl
from jax.experimental.pallas import tpu as pltpu
from jax.sharding import PartitionSpec as P

SEQS_DEV = 2


def conv_positions(values, taps):
    width = values.shape[1]
    blocks = values.reshape(SEQS_DEV, -1, width)
    length = blocks.shape[1]
    padded = jnp.pad(blocks, ((0, 0), (2, 0), (0, 0)))
    result = (
        padded[:, 0:length] * taps[0]
        + padded[:, 1 : length + 1] * taps[1]
        + padded[:, 2 : length + 2] * taps[2]
    )
    return result.reshape(-1, width)


def rms_norm(stream, gain):
    values = stream.astype(jnp.float32)
    scale = lax.rsqrt(jnp.mean(values * values, axis=-1, keepdims=True) + 1e-06)
    return (values * scale * gain).astype(jnp.bfloat16)


def on_device(
    tokens,
    mix_gain,
    w_signal,
    w_outer_gate,
    w_inner_gate,
    mix_taps,
    w_mix_out,
    ffn_gain,
    w_gate,
    w_value,
    up_taps,
    up_bias,
    w_down,
):
    whole = lax.all_gather(tokens, "tp", axis=1, tiled=True)
    normed = rms_norm(whole, mix_gain)
    pieces = (
        lax.all_gather(w_signal, "fs", axis=0, tiled=True),
        lax.all_gather(w_outer_gate, "fs", axis=0, tiled=True),
        lax.all_gather(w_inner_gate, "fs", axis=0, tiled=True),
    )
    columns = normed
    signal, outer, inner = tuple(
        (jnp.dot(columns, piece, preferred_element_type=jnp.float32) for piece in pieces)
    )
    signal = signal.astype(jnp.bfloat16).astype(jnp.float32)
    outer = outer.astype(jnp.bfloat16).astype(jnp.float32)
    inner = inner.astype(jnp.bfloat16).astype(jnp.float32)
    mixed = (outer * conv_positions(inner * signal, mix_taps)).astype(jnp.bfloat16)
    mix_terms = jnp.dot(
        mixed,
        lax.all_gather(w_mix_out, "fs", axis=1, tiled=True),
        preferred_element_type=jnp.float32,
    )
    mix_sum = lax.psum_scatter(
        mix_terms.astype(jnp.bfloat16), "tp", scatter_dimension=1, tiled=True
    ).astype(jnp.float32)
    resid = (tokens.astype(jnp.float32) + mix_sum).astype(jnp.bfloat16)
    whole_ffn = lax.all_gather(resid, "tp", axis=1, tiled=True)
    normed_ffn = rms_norm(whole_ffn, ffn_gain)
    pieces = (
        lax.all_gather(w_gate, "fs", axis=0, tiled=True),
        lax.all_gather(w_value, "fs", axis=0, tiled=True),
    )
    columns = normed_ffn
    gate = jnp.dot(columns, pieces[0], preferred_element_type=jnp.float32)
    value = jnp.dot(columns, pieces[1], preferred_element_type=jnp.float32)
    gate = gate.astype(jnp.bfloat16).astype(jnp.float32)
    value = value.astype(jnp.bfloat16).astype(jnp.float32)
    gate_conv = conv_positions(gate, up_taps[0]) + up_bias[0]
    value_conv = conv_positions(value, up_taps[1]) + up_bias[1]
    hidden = (jax.nn.silu(gate_conv) * value_conv).astype(jnp.bfloat16)
    ffn_terms = jnp.dot(
        hidden, lax.all_gather(w_down, "fs", axis=1, tiled=True), preferred_element_type=jnp.float32
    )
    ffn_sum = lax.psum_scatter(
        ffn_terms.astype(jnp.bfloat16), "tp", scatter_dimension=1, tiled=True
    ).astype(jnp.float32)
    return (resid.astype(jnp.float32) + ffn_sum).astype(jnp.bfloat16)


MESH = pl.DeviceIdType.MESH
UP, DOWN = 0, 1
LANES = 128


def shifted(values, by, length):
    rolled = pltpu.roll(values, by, 0)
    position = lax.rem(lax.broadcasted_iota(jnp.int32, values.shape, 0), length)
    return jnp.where(position < by, 0.0, rolled)


def conv_rows(values, taps, length):
    return (
        shifted(values, 2, length) * taps[0:1]
        + shifted(values, 1, length) * taps[1:2]
        + values * taps[2:3]
    )


def layer_kernel(
    n_fs,
    n_tp,
    tokens,
    mix_gain,
    w_signal,
    w_outer_gate,
    w_inner_gate,
    mix_taps,
    w_mix_out,
    ffn_gain,
    w_gate,
    w_value,
    up_taps,
    up_bias,
    w_down,
    out,
    mix_in,
    mix_out,
    ffn_in,
    ffn_out,
    tok,
    res,
    normed,
    hidden,
    part_mix,
    mix_core,
    mix_x_sum,
    mix_x_got,
    mix_z_sum,
    mix_z_got,
    part_ffn,
    got_core,
    sum_x,
    got_x,
    sum_z,
    got_z,
    z_send,
    z_recv,
    y_send,
    y_recv,
    load_sem,
    all_send,
    all_recv,
    mix_core_send,
    mix_core_recv,
    mix_x_send,
    mix_x_recv,
    core_send,
    core_recv,
    x_send,
    x_recv,
    pair_send,
    pair_recv,
):
    g, j, k = lax.axis_index("grp"), lax.axis_index("fs"), lax.axis_index("tp")
    rows, own_cols = tokens.shape
    length = rows // SEQS_DEV
    shard, chans = w_signal.shape
    half, unit_chans = shard // 2, chans // 2
    units = w_gate.shape[1] // 2
    n_in, n_out = units // LANES, shard // LANES
    n_x = n_tp // 2
    x, c = k // 2, lax.rem(k, 2)
    core = k + 1 - 2 * c
    p = lax.rem(j, 2)
    pair = j + 1 - 2 * p
    inward = jnp.where(j < n_fs // 2, 1, n_fs - 1)
    at_end = (j == 0) | (j == n_fs - 1)

    MINE, THEIRS = 0, 1

    def held_rows(o, h=None):
        side = p if o == MINE else 1 - p
        if h is None:
            return pl.ds(pl.multiple_of(side * rows, rows), rows)
        return pl.ds(pl.multiple_of(side * rows + h * length, length), length)

    def in_half(h):
        return slice(h * length, (h + 1) * length)

    mix = ("mix", 0)
    order = [mix, *(("in", t) for t in range(n_in)), *(("out", u) for u in range(n_out))]

    def other(d):
        return lax.rem(j + inward * d, n_fs)

    def sources(stage, q, side):
        kind, i = stage
        at_rows = pl.ds(pl.multiple_of(side * half, half), half)
        if kind == "mix":
            lanes = pl.ds(pl.multiple_of(q * unit_chans, unit_chans), unit_chans)
            tall = unit_chans // 2
            at = pl.ds(pl.multiple_of((q * 2 + side) * tall, tall), tall)
            refs = [ref.at[at_rows, lanes] for ref in (w_signal, w_outer_gate, w_inner_gate)]
            return [*refs, w_mix_out.at[at, :]]
        if kind == "in":
            lanes = pl.ds(pl.multiple_of(q * units + i * LANES, LANES), LANES)
            return [w_gate.at[at_rows, lanes], w_value.at[at_rows, lanes]]
        tall = units // 2
        at = pl.ds(pl.multiple_of((q * 2 + side) * tall, tall), tall)
        return [w_down.at[at, pl.ds(i * LANES, LANES)]]

    def places(stage, source, side, whole):
        kind, i = stage
        at_rows = pl.ds(pl.multiple_of((source * 2 + side) * half, half), half)
        if kind == "mix":
            tall = unit_chans // 2
            at = pl.ds(pl.multiple_of(side * tall, tall), tall)
            outs = mix_out.at[source, at, :]
            if whole:
                return [mix_in.at[at_rows, :], outs]
            lanes = [pl.ds(b * unit_chans, unit_chans) for b in range(3)]
            return [*(mix_in.at[at_rows, lane] for lane in lanes), outs]
        if kind == "in":
            if whole:
                return [ffn_in.at[i, at_rows, :]]
            return [ffn_in.at[i, at_rows, pl.ds(b * LANES, LANES)] for b in (0, 1)]
        tall = units // 2
        at = pl.ds(pl.multiple_of(side * tall, tall), tall)
        lanes = pl.ds(pl.multiple_of(source * LANES, LANES), LANES)
        return [ffn_out.at[i, at, lanes]]

    def slot(stage, i, wide):
        kind, at = stage
        if kind == "mix":
            return i
        if kind == "in":
            return (4 + 2 * at + i) if wide else 2 + at
        return 4 + 2 * n_in + at if wide else 2 + n_in + at

    def z_sends(s, d):
        to = other(d)
        return [
            pltpu.make_async_remote_copy(
                src_ref=src,
                dst_ref=dst,
                send_sem=z_send.at[slot(s, i, True), to],
                recv_sem=z_recv.at[slot(s, i, True), j],
                device_id={"fs": to},
                device_id_type=MESH,
            )
            for i, (src, dst) in enumerate(
                zip(sources(s, lax.rem(to, 2), g), places(s, j, g, False))
            )
        ]

    def z_takes(s, d):
        source = other(d)
        return [
            pltpu.make_async_remote_copy(
                src_ref=dst,
                dst_ref=dst,
                send_sem=z_send.at[slot(s, i, True), source],
                recv_sem=z_recv.at[slot(s, i, True), source],
                device_id={"fs": source},
                device_id_type=MESH,
            )
            for i, dst in enumerate(places(s, source, g, False))
        ]

    def y_copies(s, d, side):
        source = other(d)
        return [
            pltpu.make_async_remote_copy(
                src_ref=view,
                dst_ref=view,
                send_sem=y_send.at[slot(s, i, False), source],
                recv_sem=y_recv.at[slot(s, i, False), source],
                device_id={"grp": 1 - g},
                device_id_type=MESH,
            )
            for i, view in enumerate(places(s, source, side, True))
        ]

    def start(copies):
        for copy in copies:
            copy.start()

    def wait_recv(copies):
        for copy in copies:
            copy.wait_recv()

    def wait_send(copies):
        for copy in copies:
            copy.wait_send()

    def send(s, ds):
        for d in ds:
            start(z_sends(s, d))

    def relay(s, d):
        wait_recv(z_takes(s, d))
        start(y_copies(s, d, g))

    def relay_all(s):
        for d in range(1, n_fs):
            relay(s, d)

    def arrived(s):
        for d in range(1, n_fs):
            wait_recv(y_copies(s, d, 1 - g))

    def to_tp(src, dst, send_sem, recv_sem, to):
        return pltpu.make_async_remote_copy(
            src_ref=src,
            dst_ref=dst,
            send_sem=send_sem,
            recv_sem=recv_sem,
            device_id={"tp": to},
            device_id_type=MESH,
        )

    def all_copies(buffer, i, at, kind):
        copies = []
        for dx in range(n_x):
            there = lax.rem(x + dx, n_x)
            if kind == "over":
                if dx:
                    view = buffer.at[k, at]
                    sems = all_send.at[i, 0, dx], all_recv.at[i, 0, dx]
                    copies.append(to_tp(view, view, *sems, there * 2 + c))
            else:
                back = lax.rem(x + n_x - dx, n_x) * 2
                seen = back + c if kind == "pass" else back + 1 - c
                view = buffer.at[seen, at]
                sems = all_send.at[i, 1, dx], all_recv.at[i, 1, dx]
                copies.append(to_tp(view, view, *sems, core))
        return copies

    def all_begin(buffer, i, at):
        start(all_copies(buffer, i, at, "over"))
        all_copies(buffer, i, at, "pass")[0].start()

    def all_middle(buffer, i, at):
        passed = all_copies(buffer, i, at, "pass")
        for dx in range(1, n_x):
            view = buffer.at[lax.rem(x + n_x - dx, n_x) * 2 + c, at]
            to_tp(view, view, all_send.at[i, 0, dx], all_recv.at[i, 0, dx], core).wait_recv()
            passed[dx].start()

    def all_end(buffer, i, at):
        wait_recv(all_copies(buffer, i, at, "take"))

    def to_pair(i, src, dst):
        return pltpu.make_async_remote_copy(
            src_ref=src,
            dst_ref=dst,
            send_sem=pair_send.at[i],
            recv_sem=pair_recv.at[i],
            device_id={"fs": pair},
            device_id_type=MESH,
        )

    halves = range(SEQS_DEV)
    mine, theirs = held_rows(MINE), held_rows(THEIRS)

    def tok_swap(at):
        return to_pair(0, tok.at[k, at], tok.at[k, at])

    def res_swap(o, h):
        view = res.at[k, held_rows(o, h)]
        return to_pair(1 + h, view, view)

    def mix_swap(h):
        return to_pair(1 + SEQS_DEV + h, mix_z_sum.at[h], mix_z_got.at[h])

    def back(u):
        return to_pair(1 + 2 * SEQS_DEV + u, sum_z.at[u], got_z.at[u])

    barrier = pltpu.get_barrier_semaphore()
    for d in range(1, n_fs):
        to = lax.rem(j + d, n_fs)
        pl.semaphore_signal(barrier, inc=1, device_id={"fs": to}, device_id_type=MESH)
    pl.semaphore_signal(barrier, inc=1, device_id={"grp": 1 - g}, device_id_type=MESH)
    for d in range(1, n_tp):
        to = lax.rem(k + d, n_tp)
        pl.semaphore_signal(barrier, inc=1, device_id={"tp": to}, device_id_type=MESH)

    loads = [pltpu.make_async_copy(tokens, tok.at[k, mine], load_sem.at[0])]
    own_rows = pl.ds(pl.multiple_of(j * shard, shard), shard)
    own_lanes = pl.ds(pl.multiple_of(j * LANES, LANES), LANES)
    at_chans = pl.ds(pl.multiple_of(p * unit_chans, unit_chans), unit_chans)
    at_units = pl.ds(pl.multiple_of(p * units, units), units)

    def load(src, dst):
        loads.append(pltpu.make_async_copy(src, dst, load_sem.at[len(loads)]))

    for i, ref in enumerate((w_signal, w_outer_gate, w_inner_gate)):
        lanes = pl.ds(i * unit_chans, unit_chans)
        load(ref.at[:, at_chans], mix_in.at[own_rows, lanes])
    load(w_mix_out.at[at_chans, :], mix_out.at[j])
    for t in range(n_in):
        lanes = pl.ds(pl.multiple_of(p * units + t * LANES, LANES), LANES)
        for i, ref in enumerate((w_gate, w_value)):
            load(ref.at[:, lanes], ffn_in.at[t, own_rows, pl.ds(i * LANES, LANES)])
    for u in range(n_out):
        load(w_down.at[at_units, pl.ds(u * LANES, LANES)], ffn_out.at[u, :, own_lanes])
    start(loads)
    loads[0].wait()
    pl.semaphore_wait(barrier, n_fs - 1 + 1 + n_tp - 1)

    tok_swap(mine).start()
    all_begin(tok, 0, mine)
    send(mix, (*range(2, n_fs - 1), n_fs - 1, 1))
    for copy in loads[1:]:
        copy.wait()

    def norm(buffer, at, gain):
        count = at.size
        squares = jnp.zeros((count, 1), jnp.float32)
        for b in range(n_tp):
            values = buffer[b, at, :].astype(jnp.float32)
            squares = squares + jnp.sum(values * values, axis=-1, keepdims=True)
        scale = lax.rsqrt(squares / (n_tp * own_cols) + 1e-06)
        for b in range(n_tp):
            cut = slice(b * own_cols, (b + 1) * own_cols)
            values = buffer[b, at, :].astype(jnp.float32)
            normed[at, cut] = (values * scale * gain[:, cut]).astype(jnp.bfloat16)

    all_middle(tok, 0, mine)
    tok_swap(theirs).wait_recv()
    all_begin(tok, 1, theirs)
    relay(mix, 1)
    all_end(tok, 0, mine)
    norm(tok, mine, mix_gain)
    relay(mix, 2)
    all_middle(tok, 1, theirs)
    for d in range(3, n_fs):
        relay(mix, d)

    eager, late = range(1, n_fs - 1), (n_fs - 1,)

    @pl.when(jnp.logical_not(at_end))
    def _():
        for s in order[1:]:
            send(s, eager)
        for s in order[1:3]:
            send(s, late)

    @pl.when(at_end)
    def _():
        for s in order[1:3]:
            send(s, (*eager, *late))

    all_end(tok, 1, theirs)
    norm(tok, theirs, mix_gain)
    arrived(mix)

    taps = mix_taps[:, at_chans]

    def mix_core_copy(o, dx):
        there = lax.rem(x + dx, n_x)
        return to_tp(
            part_mix.at[o, there * 2 + 1 - c],
            mix_core.at[o, there],
            mix_core_send.at[o, dx],
            mix_core_recv.at[o, dx],
            core,
        )

    def mix_x_copy(o, h, dx):
        to = lax.rem(x + dx, n_x) * 2 + c
        return to_tp(
            mix_x_sum.at[o, h, dx],
            mix_x_got.at[o, h, dx],
            mix_x_send.at[o, h, dx],
            mix_x_recv.at[o, h, dx],
            to,
        )

    def mix_chip_sum(o, h, dx):
        there = lax.rem(x + dx, n_x)
        cut = in_half(h)
        near = part_mix[o, there * 2 + c, cut, :].astype(jnp.float32)
        return near + mix_core[o, there, cut, :].astype(jnp.float32)

    def mix_place_sum(o, h):
        value = mix_chip_sum(o, h, 0)
        for dx in range(1, n_x):
            value = value + mix_x_got[o, h, dx].astype(jnp.float32)
        return value

    for o, at in ((THEIRS, theirs), (MINE, mine)):
        both = jnp.dot(normed[at, :], mix_in[...], preferred_element_type=jnp.float32)
        both = both.astype(jnp.bfloat16).astype(jnp.float32)
        gated = both[:, 2 * unit_chans :] * both[:, :unit_chans]
        conv = conv_rows(gated, taps, length)
        mixed = (both[:, unit_chans : 2 * unit_chans] * conv).astype(jnp.bfloat16)
        for b in range(n_fs):
            terms = jnp.dot(mixed, mix_out[b], preferred_element_type=jnp.float32)
            part_mix[o, b] = terms.astype(jnp.bfloat16)
        for dx in (*range(1, n_x), 0):
            mix_core_copy(o, dx).start()

    for o in (THEIRS, MINE):
        for dx in range(1, n_x):
            mix_core_copy(o, dx).wait_recv()
            for h in halves:
                mix_x_sum[o, h, dx] = mix_chip_sum(o, h, dx).astype(jnp.bfloat16)
                mix_x_copy(o, h, dx).start()
        mix_core_copy(o, 0).wait_recv()
    relay_all(order[1])
    for h in halves:
        for dx in range(1, n_x):
            mix_x_copy(THEIRS, h, dx).wait_recv()
        mix_z_sum[h] = mix_place_sum(THEIRS, h).astype(jnp.bfloat16)
        mix_swap(h).start()

    def late_sends(stages):
        @pl.when(jnp.logical_not(at_end))
        def _():
            for s in stages:
                send(s, late)

        @pl.when(at_end)
        def _():
            for s in stages:
                send(s, (*eager, *late))

    late_sends(order[3:4])
    relay_all(order[2])
    for h in halves:
        for dx in range(1, n_x):
            mix_x_copy(MINE, h, dx).wait_recv()
        mix_swap(h).wait_recv()
        mixer = mix_place_sum(MINE, h) + mix_z_got[h].astype(jnp.float32)
        at = held_rows(MINE, h)
        res[k, at, :] = (tok[k, at, :].astype(jnp.float32) + mixer).astype(jnp.bfloat16)
        res_swap(MINE, h).start()
        all_begin(res, 2 + h, at)
    late_sends(order[4:])

    relay_all(order[3])
    for h in halves:
        all_middle(res, 2 + h, held_rows(MINE, h))
    for h in halves:
        res_swap(THEIRS, h).wait_recv()
        all_begin(res, 2 + SEQS_DEV + h, held_rows(THEIRS, h))
    for h in halves:
        all_end(res, 2 + h, held_rows(MINE, h))
        norm(res, held_rows(MINE, h), ffn_gain)
    for h in halves:
        all_middle(res, 2 + SEQS_DEV + h, held_rows(THEIRS, h))
    relay_all(order[4])
    for h in halves:
        all_end(res, 2 + SEQS_DEV + h, held_rows(THEIRS, h))
        norm(res, held_rows(THEIRS, h), ffn_gain)

    def feed(t):
        arrived(("in", t))
        cut = pl.ds(pl.multiple_of(p * units + t * LANES, LANES), LANES)
        both = jnp.dot(normed[...], ffn_in[t], preferred_element_type=jnp.float32)
        both = both.astype(jnp.bfloat16).astype(jnp.float32)
        gate = conv_rows(both[:, :LANES], up_taps[0, :, cut], length) + up_bias[0:1, cut]
        value = conv_rows(both[:, LANES:], up_taps[1, :, cut], length) + up_bias[1:2, cut]
        unit = (gate / (1.0 + jnp.exp(-gate)) * value).astype(jnp.bfloat16)
        hidden[:, pl.ds(pl.multiple_of(t * LANES, LANES), LANES)] = unit

    beside = {2: 5, 3: 6, 4: 7}

    @pl.loop(0, n_in)
    def _(t):
        for at, index in beside.items():

            @pl.when(t == at)
            def _():
                relay_all(order[index])

        feed(t)

    def core_copy(u, dx):
        there = lax.rem(x + dx, n_x)
        return to_tp(
            part_ffn.at[u, :, there * 2 + 1 - c],
            got_core.at[u, :, there],
            core_send.at[u, dx],
            core_recv.at[u, dx],
            core,
        )

    def x_copy(u, dx):
        to = lax.rem(x + dx, n_x) * 2 + c
        return to_tp(sum_x.at[u, dx], got_x.at[u, dx], x_send.at[u, dx], x_recv.at[u, dx], to)

    def chip_sum(u, o, dx):
        there = lax.rem(x + dx, n_x)
        mine_there = part_ffn[u, o, there * 2 + c].astype(jnp.float32)
        return mine_there + got_core[u, o, there].astype(jnp.float32)

    def place_sum(u, o):
        value = chip_sum(u, o, 0)
        for dx in range(1, n_x):
            value = value + got_x[u, dx, o].astype(jnp.float32)
        return value

    def down(u):
        arrived(("out", u))
        for o, at in enumerate((theirs, mine)):
            terms = jnp.dot(hidden[at, :], ffn_out[u], preferred_element_type=jnp.float32)
            for b in range(n_tp):
                part_ffn[u, o, b] = terms[:, b * LANES : (b + 1) * LANES].astype(jnp.bfloat16)
        for dx in (*range(1, n_x), 0):
            core_copy(u, dx).start()

    def over_x(u):
        for dx in range(1, n_x):
            core_copy(u, dx).wait_recv()
            for o in (0, 1):
                sum_x[u, dx, o] = chip_sum(u, o, dx).astype(jnp.bfloat16)
            x_copy(u, dx).start()

    def over_z(u):
        core_copy(u, 0).wait_recv()
        for dx in range(1, n_x):
            x_copy(u, dx).wait_recv()
        sum_z[u] = place_sum(u, 0).astype(jnp.bfloat16)
        back(u).start()

    for u in range(n_out):
        if 8 + u < len(order):
            relay_all(order[8 + u])
        down(u)
        if u >= 1:
            over_x(u - 1)
        if u >= 2:
            over_z(u - 2)
    over_x(n_out - 1)
    for u in range(max(n_out - 2, 0), n_out):
        over_z(u)
    for u in range(n_out):
        cut = slice(u * LANES, (u + 1) * LANES)
        value = res[k, mine, cut].astype(jnp.float32) + place_sum(u, 1)
        back(u).wait_recv()
        out[:, cut] = (value + got_z[u].astype(jnp.float32)).astype(jnp.bfloat16)

    tok_swap(mine).wait_send()
    gathers = [(tok, 0, mine), (tok, 1, theirs)]
    for h in halves:
        gathers.append((res, 2 + h, held_rows(MINE, h)))
        gathers.append((res, 2 + SEQS_DEV + h, held_rows(THEIRS, h)))
        res_swap(MINE, h).wait_send()
        mix_swap(h).wait_send()
    for gather in gathers:
        wait_send(all_copies(*gather, "over"))
        wait_send(all_copies(*gather, "pass"))
    for o in (MINE, THEIRS):
        for dx in range(n_x):
            mix_core_copy(o, dx).wait_send()
        for dx in range(1, n_x):
            for h in halves:
                mix_x_copy(o, h, dx).wait_send()
    for u in range(n_out):
        for dx in range(n_x):
            core_copy(u, dx).wait_send()
        for dx in range(1, n_x):
            x_copy(u, dx).wait_send()
        back(u).wait_send()

    for s in order:
        for d in range(1, n_fs):
            wait_send(z_sends(s, d))
            wait_send(y_copies(s, d, g))


def fused(n_fs, n_tp, *args):
    tokens, w_signal, w_gate = args[0], args[2], args[8]
    rows, cols = tokens.shape
    shard, chans = w_signal.shape
    units = w_gate.shape[1] // 2
    n_in, n_out = units // LANES, shard // LANES
    width = n_fs * shard
    args = list(args)
    args[1], args[7] = args[1].reshape(1, -1), args[7].reshape(1, -1)
    in_vmem = {1, 5, 7, 10, 11}
    n_x = n_tp // 2
    length = rows // SEQS_DEV
    dma = pltpu.SemaphoreType.DMA

    def held(*shape):
        return pltpu.VMEM(shape, jnp.bfloat16)

    return pl.pallas_call(
        functools.partial(layer_kernel, n_fs, n_tp),
        out_shape=jax.ShapeDtypeStruct((rows, cols), jnp.bfloat16),
        in_specs=[
            pl.BlockSpec(memory_space=pltpu.VMEM if i in in_vmem else pl.ANY)
            for i in range(len(args))
        ],
        out_specs=pl.BlockSpec(memory_space=pltpu.VMEM),
        scratch_shapes=[
            held(width, 3 * (chans // 2)),
            held(n_fs, chans // 2, shard),
            held(n_in, width, 2 * LANES),
            held(n_out, units, n_fs * LANES),
            held(n_tp, 2 * rows, cols),
            held(n_tp, 2 * rows, cols),
            held(2 * rows, width),
            held(2 * rows, units),
            held(2, n_tp, rows, cols),
            held(2, n_x, rows, cols),
            held(2, SEQS_DEV, n_x, length, cols),
            held(2, SEQS_DEV, n_x, length, cols),
            held(SEQS_DEV, length, cols),
            held(SEQS_DEV, length, cols),
            held(n_out, 2, n_tp, rows, LANES),
            held(n_out, 2, n_x, rows, LANES),
            held(n_out, n_x, 2, rows, LANES),
            held(n_out, n_x, 2, rows, LANES),
            held(n_out, rows, LANES),
            held(n_out, rows, LANES),
            dma((4 + 2 * n_in + n_out, n_fs)),
            dma((4 + 2 * n_in + n_out, n_fs)),
            dma((2 + n_in + n_out, n_fs)),
            dma((2 + n_in + n_out, n_fs)),
            dma((5 + 2 * n_in + n_out,)),
            dma((2 + 2 * SEQS_DEV, 2, n_x)),
            dma((2 + 2 * SEQS_DEV, 2, n_x)),
            dma((2, n_x)),
            dma((2, n_x)),
            dma((2, SEQS_DEV, n_x)),
            dma((2, SEQS_DEV, n_x)),
            dma((n_out, n_x)),
            dma((n_out, n_x)),
            dma((n_out, n_x)),
            dma((n_out, n_x)),
            dma((1 + 2 * SEQS_DEV + n_out,)),
            dma((1 + 2 * SEQS_DEV + n_out,)),
        ],
        compiler_params=pltpu.CompilerParams(
            collective_id=0, has_side_effects=True, vmem_limit_bytes=62 * 1024 * 1024
        ),
    )(*args)


def solution(mesh):
    n_fs, n_tp = mesh.shape["fs"], mesh.shape["tp"]
    body = functools.partial(fused, n_fs, n_tp)
    if n_fs > 8 or n_fs != n_tp or n_fs % 2 or mesh.shape["grp"] != 2:
        body = on_device
    placed = (
        P(("grp", "fs"), "tp"),
        P(),
        P("fs", "tp"),
        P("fs", "tp"),
        P("fs", "tp"),
        P(None, "tp"),
        P("tp", "fs"),
        P(),
        P("fs", "tp"),
        P("fs", "tp"),
        P(None, None, "tp"),
        P(None, "tp"),
        P("tp", "fs"),
    )
    return jax.shard_map(
        body, mesh=mesh, in_specs=placed, out_specs=P(("grp", "fs"), "tp"), check_vma=False
    )
```

time: 176 us -> 163 us (0.926)
  Pallas kernels: 172 us -> 159 us
    pallas_call x1, Pallas kernels: 172 us -> 159 us  [fused(): pl.pallas_call(functools.partial(layer_kernel, n_fs, n_tp), out_shape=jax...]
where the time goes in v1:
time: 163 us; the launch traced here: 162 us
  Pallas kernels  159 us (98%)
  local copies, waits for them, and re-layouts  3.15 us (2%)
    pallas_call x1, Pallas kernels, fused(): pl.pallas_call(functools.partial(layer_kernel, n_fs, n_tp), out_shape=jax...  159 us

profile of v1, /device:TPU:0, one launch (start us, length us, event | category | flops | bytes accessed | tf_op | source)
XLA Modules:
  0.0 162.3 jit_solution(477877091370383090)
XLA Ops:
  0.0 1.4 copy.14.up_taps
  1.4 159.1 %shard_map.127 = bf16[384,512]{1,0:T(8,128)(2,1)} custom-call(bf16[384,512]{1,0:T(8,128)(2,1)} %tokens.1, f32[1,2048]{1,0:T(1,128)} %bitcast.2, bf16[512,256]{1,0:T(8,128)(2,1)} %w_signal.1, bf16[512,256]{1,0:T(8,128)(2,1)} %w_outer_gate.1, bf16[512,256]{1,0:T(8,128)(2,1)} %w_inner_gate.1, f32[3,256]{1,0:T(4,128)} %mix_taps.1, bf16[256,512]{1,0:T(8,128)(2,1)} %w_mix_out.1, ...), custom_call_target="tpu_custom_call" | custom-call | tf_op jit(solution)/shard_map/pallas_call | solution.py:695
  160.5 1.8 %copy.16 = bf16[384,512]{1,0:T(8,128)(2,1)} copy(bf16[384,512]{1,0:T(8,128)(2,1)} %shard_map.127) | data formatting | bytes 786432

commit v2 on v1

--- a/solution.py
+++ b/solution.py
@@ -104,9 +104,9 @@
 
 def conv_rows(values, taps, length):
     return (
-        shifted(values, 2, length) * taps[0:1]
-        + shifted(values, 1, length) * taps[1:2]
-        + values * taps[2:3]
+        shifted(values, 2, length) * taps[0]
+        + shifted(values, 1, length) * taps[1]
+        + values * taps[2]
     )
 
 
@@ -149,6 +149,7 @@
     got_z,
     z_send,
     z_recv,
+    f_send,
     y_send,
     y_recv,
     load_sem,
@@ -233,56 +234,83 @@
         lanes = pl.ds(pl.multiple_of(source * LANES, LANES), LANES)
         return [ffn_out.at[i, at, lanes]]
 
-    def slot(stage, i, wide):
+    def slot(stage, i):
         kind, at = stage
         if kind == "mix":
             return i
-        if kind == "in":
-            return (4 + 2 * at + i) if wide else 2 + at
-        return 4 + 2 * n_in + at if wide else 2 + n_in + at
+        return 2 + at if kind == "in" else 2 + n_in + at
+
+    def group(stage, i):
+        kind, _ = stage
+        return i if kind == "mix" else {"in": 2, "out": 3}[kind]
+
+    def to_fs(src, dst, send_sem, recv_sem, to):
+        return pltpu.make_async_remote_copy(
+            src_ref=src,
+            dst_ref=dst,
+            send_sem=send_sem,
+            recv_sem=recv_sem,
+            device_id={"fs": to},
+            device_id_type=MESH,
+        )
 
     def z_sends(s, d):
         to = other(d)
-        return [
-            pltpu.make_async_remote_copy(
-                src_ref=src,
-                dst_ref=dst,
-                send_sem=z_send.at[slot(s, i, True), to],
-                recv_sem=z_recv.at[slot(s, i, True), j],
-                device_id={"fs": to},
-                device_id_type=MESH,
-            )
-            for i, (src, dst) in enumerate(
-                zip(sources(s, lax.rem(to, 2), g), places(s, j, g, False))
-            )
-        ]
+        pairs = zip(sources(s, lax.rem(to, 2), g), places(s, j, g, False))
+        copies = []
+        for i, (src, dst) in enumerate(pairs):
+            wide = i // 3 if s[0] == "mix" else 0
+            sems = z_send.at[group(s, wide)], z_recv.at[slot(s, wide), j]
+            copies.append(to_fs(src, dst, *sems, to))
+        return copies
 
     def z_takes(s, d):
         source = other(d)
         return [
-            pltpu.make_async_remote_copy(
-                src_ref=dst,
-                dst_ref=dst,
-                send_sem=z_send.at[slot(s, i, True), source],
-                recv_sem=z_recv.at[slot(s, i, True), source],
-                device_id={"fs": source},
-                device_id_type=MESH,
-            )
-            for i, dst in enumerate(places(s, source, g, False))
+            to_fs(view, view, z_send.at[group(s, i)], z_recv.at[slot(s, i), source], source)
+            for i, view in enumerate(places(s, source, g, True))
         ]
 
-    def y_copies(s, d, side):
-        source = other(d)
+    def z_forwards(s):
+        source = other(n_fs - 1)
         return [
-            pltpu.make_async_remote_copy(
-                src_ref=view,
-                dst_ref=view,
-                send_sem=y_send.at[slot(s, i, False), source],
-                recv_sem=y_recv.at[slot(s, i, False), source],
-                device_id={"grp": 1 - g},
-                device_id_type=MESH,
-            )
-            for i, view in enumerate(places(s, source, side, True))
+            to_fs(view, view, f_send.at[group(s, i)], z_recv.at[slot(s, i), source], other(n_fs - 2))
+            for i, view in enumerate(places(s, source, g, True))
+        ]
+
+    def to_y(src, dst, send_sem, recv_sem):
+        return pltpu.make_async_remote_copy(
+            src_ref=src,
+            dst_ref=dst,
+            send_sem=send_sem,
+            recv_sem=recv_sem,
+            device_id={"grp": 1 - g},
+            device_id_type=MESH,
+        )
+
+    def y_copies(s, d):
+        return [
+            to_y(view, view, y_send.at[group(s, i)], y_recv.at[slot(s, i)])
+            for i, view in enumerate(places(s, other(d), g, True))
+        ]
+
+    n_from = n_fs - 1
+
+    def sums(stage):
+        kind, i = stage
+        if kind == "mix":
+            some = mix_out.at[pl.ds(0, n_from), pl.ds(0, unit_chans // 2), :]
+            return [mix_in.at[pl.ds(0, n_from * half), :], some]
+        if kind == "in":
+            return [ffn_in.at[i, pl.ds(0, n_from * half), :]]
+        return [ffn_out.at[i, pl.ds(0, units // 2), pl.ds(0, n_from * LANES)]]
+
+    def all_sums(count):
+        return [
+            mix_in.at[pl.ds(0, count * half), :],
+            mix_out.at[pl.ds(0, count), pl.ds(0, unit_chans // 2), :],
+            ffn_in.at[:, pl.ds(0, count * half), :],
+            ffn_out.at[:, pl.ds(0, units // 2), pl.ds(0, count * LANES)],
         ]
 
     def start(copies):
@@ -301,17 +329,32 @@
         for d in ds:
             start(z_sends(s, d))
 
+    straight, last = range(1, n_fs - 1), n_fs - 1
+
     def relay(s, d):
         wait_recv(z_takes(s, d))
-        start(y_copies(s, d, g))
-
-    def relay_all(s):
-        for d in range(1, n_fs):
-            relay(s, d)
+        start(y_copies(s, d))
+
+    def relay_all(s, following=()):
+        relay(s, 1)
+
+        @pl.when(at_end)
+        def _():
+            for d in range(2, n_fs):
+                relay(s, d)
+
+        @pl.when(jnp.logical_not(at_end))
+        def _():
+            relay(s, last)
+            start(z_forwards(s))
+            for later in following:
+                send(later, straight)
+            for d in range(2, n_fs - 1):
+                relay(s, d)
 
     def arrived(s):
-        for d in range(1, n_fs):
-            wait_recv(y_copies(s, d, 1 - g))
+        for i, view in enumerate(sums(s)):
+            to_y(view, view, y_send.at[group(s, i)], y_recv.at[slot(s, i)]).wait_recv()
 
     def to_tp(src, dst, send_sem, recv_sem, to):
         return pltpu.make_async_remote_copy(
@@ -324,20 +367,19 @@
         )
 
     def all_copies(buffer, i, at, kind):
+        sent = all_send.at[0 if i < 2 else 1]
         copies = []
         for dx in range(n_x):
             there = lax.rem(x + dx, n_x)
             if kind == "over":
                 if dx:
                     view = buffer.at[k, at]
-                    sems = all_send.at[i, 0, dx], all_recv.at[i, 0, dx]
-                    copies.append(to_tp(view, view, *sems, there * 2 + c))
+                    copies.append(to_tp(view, view, sent, all_recv.at[i, dx - 1], there * 2 + c))
             else:
                 back = lax.rem(x + n_x - dx, n_x) * 2
                 seen = back + c if kind == "pass" else back + 1 - c
                 view = buffer.at[seen, at]
-                sems = all_send.at[i, 1, dx], all_recv.at[i, 1, dx]
-                copies.append(to_tp(view, view, *sems, core))
+                copies.append(to_tp(view, view, sent, all_recv.at[i, n_x - 1 + dx], core))
         return copies
 
     def all_begin(buffer, i, at):
@@ -348,7 +390,8 @@
         passed = all_copies(buffer, i, at, "pass")
         for dx in range(1, n_x):
             view = buffer.at[lax.rem(x + n_x - dx, n_x) * 2 + c, at]
-            to_tp(view, view, all_send.at[i, 0, dx], all_recv.at[i, 0, dx], core).wait_recv()
+            sent = all_send.at[0 if i < 2 else 1]
+            to_tp(view, view, sent, all_recv.at[i, dx - 1], core).wait_recv()
             passed[dx].start()
 
     def all_end(buffer, i, at):
@@ -358,7 +401,7 @@
         return pltpu.make_async_remote_copy(
             src_ref=src,
             dst_ref=dst,
-            send_sem=pair_send.at[i],
+            send_sem=pair_send.at[0],
             recv_sem=pair_recv.at[i],
             device_id={"fs": pair},
             device_id_type=MESH,
@@ -389,34 +432,53 @@
         to = lax.rem(k + d, n_tp)
         pl.semaphore_signal(barrier, inc=1, device_id={"tp": to}, device_id_type=MESH)
 
-    loads = [pltpu.make_async_copy(tokens, tok.at[k, mine], load_sem.at[0])]
+    first = pltpu.make_async_copy(tokens, tok.at[k, mine], load_sem.at[4])
     own_rows = pl.ds(pl.multiple_of(j * shard, shard), shard)
     own_lanes = pl.ds(pl.multiple_of(j * LANES, LANES), LANES)
     at_chans = pl.ds(pl.multiple_of(p * unit_chans, unit_chans), unit_chans)
     at_units = pl.ds(pl.multiple_of(p * units, units), units)
 
-    def load(src, dst):
-        loads.append(pltpu.make_async_copy(src, dst, load_sem.at[len(loads)]))
-
+    def load(i, src, dst):
+        pltpu.make_async_copy(src, dst, load_sem.at[i]).start()
+
+    first.start()
     for i, ref in enumerate((w_signal, w_outer_gate, w_inner_gate)):
-        lanes = pl.ds(i * unit_chans, unit_chans)
-        load(ref.at[:, at_chans], mix_in.at[own_rows, lanes])
-    load(w_mix_out.at[at_chans, :], mix_out.at[j])
+        load(0, ref.at[:, at_chans], mix_in.at[own_rows, pl.ds(i * unit_chans, unit_chans)])
+    load(1, w_mix_out.at[at_chans, :], mix_out.at[j])
     for t in range(n_in):
         lanes = pl.ds(pl.multiple_of(p * units + t * LANES, LANES), LANES)
         for i, ref in enumerate((w_gate, w_value)):
-            load(ref.at[:, lanes], ffn_in.at[t, own_rows, pl.ds(i * LANES, LANES)])
+            load(2, ref.at[:, lanes], ffn_in.at[t, own_rows, pl.ds(i * LANES, LANES)])
     for u in range(n_out):
-        load(w_down.at[at_units, pl.ds(u * LANES, LANES)], ffn_out.at[u, :, own_lanes])
-    start(loads)
-    loads[0].wait()
-    pl.semaphore_wait(barrier, n_fs - 1 + 1 + n_tp - 1)
-
-    tok_swap(mine).start()
-    all_begin(tok, 0, mine)
-    send(mix, (*range(2, n_fs - 1), n_fs - 1, 1))
-    for copy in loads[1:]:
-        copy.wait()
+        load(3, w_down.at[at_units, pl.ds(u * LANES, LANES)], ffn_out.at[u, :, own_lanes])
+    loaded = [
+        mix_in.at[own_rows, :],
+        mix_out.at[j],
+        ffn_in.at[:, own_rows, :],
+        ffn_out.at[:, :, own_lanes],
+    ]
+    with jax.named_scope("barrier"):
+        first.wait()
+        pl.semaphore_wait(barrier, n_fs - 1 + 1 + n_tp - 1)
+
+    send(mix, (1,))
+
+    @pl.when(at_end)
+    def _():
+        tok_swap(mine).start()
+        all_begin(tok, 0, mine)
+        send(mix, range(2, n_fs - 1))
+
+    @pl.when(jnp.logical_not(at_end))
+    def _():
+        send(mix, (last,))
+        tok_swap(mine).start()
+        all_begin(tok, 0, mine)
+        send(mix, range(2, n_fs - 1))
+
+    with jax.named_scope("loads"):
+        for i, view in enumerate(loaded):
+            pltpu.make_async_copy(view, view, load_sem.at[i]).wait()
 
     def norm(buffer, at, gain):
         count = at.size
@@ -430,43 +492,60 @@
             values = buffer[b, at, :].astype(jnp.float32)
             normed[at, cut] = (values * scale * gain[:, cut]).astype(jnp.bfloat16)
 
-    all_middle(tok, 0, mine)
-    tok_swap(theirs).wait_recv()
-    all_begin(tok, 1, theirs)
-    relay(mix, 1)
-    all_end(tok, 0, mine)
-    norm(tok, mine, mix_gain)
-    relay(mix, 2)
-    all_middle(tok, 1, theirs)
-    for d in range(3, n_fs):
-        relay(mix, d)
-
-    eager, late = range(1, n_fs - 1), (n_fs - 1,)
+    with jax.named_scope("tok_mid"):
+        all_middle(tok, 0, mine)
+    with jax.named_scope("relay_mix1"):
+        relay(mix, 1)
+
+    @pl.when(at_end)
+    def _():
+        with jax.named_scope("relay_mix2"):
+            relay(mix, 2)
 
     @pl.when(jnp.logical_not(at_end))
     def _():
-        for s in order[1:]:
-            send(s, eager)
-        for s in order[1:3]:
-            send(s, late)
+        with jax.named_scope("relay_mix2"):
+            relay(mix, last)
+            start(z_forwards(mix))
+
+    with jax.named_scope("norm_mine"):
+        all_end(tok, 0, mine)
+        norm(tok, mine, mix_gain)
+    with jax.named_scope("tok_swap"):
+        tok_swap(theirs).wait_recv()
+        all_begin(tok, 1, theirs)
 
     @pl.when(at_end)
     def _():
+        with jax.named_scope("relay_mix3"):
+            relay(mix, last)
+        for s in order[1:4]:
+            send(s, straight)
+
+    @pl.when(jnp.logical_not(at_end))
+    def _():
+        with jax.named_scope("relay_mix3"):
+            relay(mix, 2)
         for s in order[1:3]:
-            send(s, (*eager, *late))
-
-    all_end(tok, 1, theirs)
-    norm(tok, theirs, mix_gain)
-    arrived(mix)
-
-    taps = mix_taps[:, at_chans]
+            send(s, straight)
+        for s in order[1:4]:
+            send(s, (last,))
+
+    with jax.named_scope("tok_theirs"):
+        all_middle(tok, 1, theirs)
+    with jax.named_scope("norm_theirs"):
+        all_end(tok, 1, theirs)
+        norm(tok, theirs, mix_gain)
+    with jax.named_scope("arrived_mix"):
+        arrived(mix)
+    taps = [mix_taps[i : i + 1, at_chans] for i in range(3)]
 
     def mix_core_copy(o, dx):
         there = lax.rem(x + dx, n_x)
         return to_tp(
             part_mix.at[o, there * 2 + 1 - c],
             mix_core.at[o, there],
-            mix_core_send.at[o, dx],
+            mix_core_send.at[0],
             mix_core_recv.at[o, dx],
             core,
         )
@@ -474,10 +553,10 @@
     def mix_x_copy(o, h, dx):
         to = lax.rem(x + dx, n_x) * 2 + c
         return to_tp(
-            mix_x_sum.at[o, h, dx],
-            mix_x_got.at[o, h, dx],
-            mix_x_send.at[o, h, dx],
-            mix_x_recv.at[o, h, dx],
+            mix_x_sum.at[o, h, dx - 1],
+            mix_x_got.at[o, h, dx - 1],
+            mix_x_send.at[0],
+            mix_x_recv.at[o, h, dx - 1],
             to,
         )
 
@@ -490,82 +569,95 @@
     def mix_place_sum(o, h):
         value = mix_chip_sum(o, h, 0)
         for dx in range(1, n_x):
-            value = value + mix_x_got[o, h, dx].astype(jnp.float32)
+            value = value + mix_x_got[o, h, dx - 1].astype(jnp.float32)
         return value
 
-    for o, at in ((THEIRS, theirs), (MINE, mine)):
-        both = jnp.dot(normed[at, :], mix_in[...], preferred_element_type=jnp.float32)
-        both = both.astype(jnp.bfloat16).astype(jnp.float32)
-        gated = both[:, 2 * unit_chans :] * both[:, :unit_chans]
-        conv = conv_rows(gated, taps, length)
-        mixed = (both[:, unit_chans : 2 * unit_chans] * conv).astype(jnp.bfloat16)
-        for b in range(n_fs):
-            terms = jnp.dot(mixed, mix_out[b], preferred_element_type=jnp.float32)
-            part_mix[o, b] = terms.astype(jnp.bfloat16)
-        for dx in (*range(1, n_x), 0):
-            mix_core_copy(o, dx).start()
-
-    for o in (THEIRS, MINE):
-        for dx in range(1, n_x):
-            mix_core_copy(o, dx).wait_recv()
-            for h in halves:
-                mix_x_sum[o, h, dx] = mix_chip_sum(o, h, dx).astype(jnp.bfloat16)
-                mix_x_copy(o, h, dx).start()
-        mix_core_copy(o, 0).wait_recv()
-    relay_all(order[1])
-    for h in halves:
-        for dx in range(1, n_x):
-            mix_x_copy(THEIRS, h, dx).wait_recv()
-        mix_z_sum[h] = mix_place_sum(THEIRS, h).astype(jnp.bfloat16)
-        mix_swap(h).start()
-
-    def late_sends(stages):
-        @pl.when(jnp.logical_not(at_end))
-        def _():
-            for s in stages:
-                send(s, late)
-
-        @pl.when(at_end)
-        def _():
-            for s in stages:
-                send(s, (*eager, *late))
-
-    late_sends(order[3:4])
-    relay_all(order[2])
-    for h in halves:
-        for dx in range(1, n_x):
-            mix_x_copy(MINE, h, dx).wait_recv()
-        mix_swap(h).wait_recv()
-        mixer = mix_place_sum(MINE, h) + mix_z_got[h].astype(jnp.float32)
-        at = held_rows(MINE, h)
-        res[k, at, :] = (tok[k, at, :].astype(jnp.float32) + mixer).astype(jnp.bfloat16)
-        res_swap(MINE, h).start()
-        all_begin(res, 2 + h, at)
-    late_sends(order[4:])
-
-    relay_all(order[3])
-    for h in halves:
-        all_middle(res, 2 + h, held_rows(MINE, h))
-    for h in halves:
-        res_swap(THEIRS, h).wait_recv()
-        all_begin(res, 2 + SEQS_DEV + h, held_rows(THEIRS, h))
-    for h in halves:
-        all_end(res, 2 + h, held_rows(MINE, h))
-        norm(res, held_rows(MINE, h), ffn_gain)
-    for h in halves:
-        all_middle(res, 2 + SEQS_DEV + h, held_rows(THEIRS, h))
-    relay_all(order[4])
-    for h in halves:
-        all_end(res, 2 + SEQS_DEV + h, held_rows(THEIRS, h))
-        norm(res, held_rows(THEIRS, h), ffn_gain)
+    with jax.named_scope("mixer"):
+        for o, at in ((THEIRS, theirs), (MINE, mine)):
+            both = jnp.dot(normed[at, :], mix_in[...], preferred_element_type=jnp.float32)
+            both = both.astype(jnp.bfloat16).astype(jnp.float32)
+            gated = both[:, 2 * unit_chans :] * both[:, :unit_chans]
+            conv = conv_rows(gated, taps, length)
+            mixed = (both[:, unit_chans : 2 * unit_chans] * conv).astype(jnp.bfloat16)
+            for b in range(n_fs):
+                terms = jnp.dot(mixed, mix_out[b], preferred_element_type=jnp.float32)
+                part_mix[o, b] = terms.astype(jnp.bfloat16)
+            for dx in (*range(1, n_x), 0):
+                mix_core_copy(o, dx).start()
+
+    with jax.named_scope("mix_core"):
+        for o in (THEIRS, MINE):
+            for dx in range(1, n_x):
+                mix_core_copy(o, dx).wait_recv()
+                for h in halves:
+                    mix_x_sum[o, h, dx - 1] = mix_chip_sum(o, h, dx).astype(jnp.bfloat16)
+                    mix_x_copy(o, h, dx).start()
+            mix_core_copy(o, 0).wait_recv()
+    with jax.named_scope("relay_in0"):
+        relay_all(order[1], order[3:4])
+    with jax.named_scope("mix_x_theirs"):
+        for h in halves:
+            for dx in range(1, n_x):
+                mix_x_copy(THEIRS, h, dx).wait_recv()
+            mix_z_sum[h] = mix_place_sum(THEIRS, h).astype(jnp.bfloat16)
+            mix_swap(h).start()
+
+    with jax.named_scope("relay_in1"):
+        relay_all(order[2], order[4:5])
+    with jax.named_scope("mix_mine"):
+        for h in halves:
+            for dx in range(1, n_x):
+                mix_x_copy(MINE, h, dx).wait_recv()
+            mix_swap(h).wait_recv()
+            mixer = mix_place_sum(MINE, h) + mix_z_got[h].astype(jnp.float32)
+            at = held_rows(MINE, h)
+            res[k, at, :] = (tok[k, at, :].astype(jnp.float32) + mixer).astype(jnp.bfloat16)
+            res_swap(MINE, h).start()
+            all_begin(res, 2 + h, at)
+
+    @pl.when(at_end)
+    def _():
+        for s in order[4:]:
+            send(s, straight)
+
+    @pl.when(jnp.logical_not(at_end))
+    def _():
+        for s in order[4:]:
+            send(s, (last,))
+
+
+    with jax.named_scope("relay_in2"):
+        relay_all(order[3], order[5:6])
+    with jax.named_scope("res_mid"):
+        for h in halves:
+            all_middle(res, 2 + h, held_rows(MINE, h))
+    with jax.named_scope("res_swap"):
+        for h in halves:
+            res_swap(THEIRS, h).wait_recv()
+            all_begin(res, 2 + SEQS_DEV + h, held_rows(THEIRS, h))
+    with jax.named_scope("res_norm"):
+        for h in halves:
+            all_end(res, 2 + h, held_rows(MINE, h))
+            norm(res, held_rows(MINE, h), ffn_gain)
+    with jax.named_scope("res_mid2"):
+        for h in halves:
+            all_middle(res, 2 + SEQS_DEV + h, held_rows(THEIRS, h))
+    with jax.named_scope("relay_in3"):
+        relay_all(order[4], order[6:7])
+    with jax.named_scope("res_norm2"):
+        for h in halves:
+            all_end(res, 2 + SEQS_DEV + h, held_rows(THEIRS, h))
+            norm(res, held_rows(THEIRS, h), ffn_gain)
 
     def feed(t):
-        arrived(("in", t))
+        with jax.named_scope("in_wait"):
+            arrived(("in", t))
         cut = pl.ds(pl.multiple_of(p * units + t * LANES, LANES), LANES)
         both = jnp.dot(normed[...], ffn_in[t], preferred_element_type=jnp.float32)
         both = both.astype(jnp.bfloat16).astype(jnp.float32)
-        gate = conv_rows(both[:, :LANES], up_taps[0, :, cut], length) + up_bias[0:1, cut]
-        value = conv_rows(both[:, LANES:], up_taps[1, :, cut], length) + up_bias[1:2, cut]
+        gate_taps, value_taps = ([up_taps[i, b : b + 1, cut] for i in range(3)] for b in (0, 1))
+        gate = conv_rows(both[:, :LANES], gate_taps, length) + up_bias[0:1, cut]
+        value = conv_rows(both[:, LANES:], value_taps, length) + up_bias[1:2, cut]
         unit = (gate / (1.0 + jnp.exp(-gate)) * value).astype(jnp.bfloat16)
         hidden[:, pl.ds(pl.multiple_of(t * LANES, LANES), LANES)] = unit
 
@@ -577,7 +669,8 @@
 
             @pl.when(t == at)
             def _():
-                relay_all(order[index])
+                with jax.named_scope("relay_out"):
+                    relay_all(order[index], order[index + 2 : index + 3])
 
         feed(t)
 
@@ -586,14 +679,15 @@
         return to_tp(
             part_ffn.at[u, :, there * 2 + 1 - c],
             got_core.at[u, :, there],
-            core_send.at[u, dx],
+            core_send.at[0],
             core_recv.at[u, dx],
             core,
         )
 
     def x_copy(u, dx):
         to = lax.rem(x + dx, n_x) * 2 + c
-        return to_tp(sum_x.at[u, dx], got_x.at[u, dx], x_send.at[u, dx], x_recv.at[u, dx], to)
+        sems = x_send.at[0], x_recv.at[u, dx - 1]
+        return to_tp(sum_x.at[u, dx - 1], got_x.at[u, dx - 1], *sems, to)
 
     def chip_sum(u, o, dx):
         there = lax.rem(x + dx, n_x)
@@ -603,11 +697,12 @@
     def place_sum(u, o):
         value = chip_sum(u, o, 0)
         for dx in range(1, n_x):
-            value = value + got_x[u, dx, o].astype(jnp.float32)
+            value = value + got_x[u, dx - 1, o].astype(jnp.float32)
         return value
 
     def down(u):
-        arrived(("out", u))
+        with jax.named_scope("out_wait"):
+            arrived(("out", u))
         for o, at in enumerate((theirs, mine)):
             terms = jnp.dot(hidden[at, :], ffn_out[u], preferred_element_type=jnp.float32)
             for b in range(n_tp):
@@ -619,7 +714,7 @@
         for dx in range(1, n_x):
             core_copy(u, dx).wait_recv()
             for o in (0, 1):
-                sum_x[u, dx, o] = chip_sum(u, o, dx).astype(jnp.bfloat16)
+                sum_x[u, dx - 1, o] = chip_sum(u, o, dx).astype(jnp.bfloat16)
             x_copy(u, dx).start()
 
     def over_z(u):
@@ -631,48 +726,55 @@
 
     for u in range(n_out):
         if 8 + u < len(order):
-            relay_all(order[8 + u])
-        down(u)
+            with jax.named_scope("relay_out2"):
+                relay_all(order[8 + u], order[10 + u : 11 + u])
+        with jax.named_scope("down"):
+            down(u)
         if u >= 1:
-            over_x(u - 1)
+            with jax.named_scope("over_x"):
+                over_x(u - 1)
         if u >= 2:
-            over_z(u - 2)
-    over_x(n_out - 1)
+            with jax.named_scope("over_z"):
+                over_z(u - 2)
+    with jax.named_scope("over_x_last"):
+        over_x(n_out - 1)
     for u in range(max(n_out - 2, 0), n_out):
-        over_z(u)
-    for u in range(n_out):
-        cut = slice(u * LANES, (u + 1) * LANES)
-        value = res[k, mine, cut].astype(jnp.float32) + place_sum(u, 1)
-        back(u).wait_recv()
-        out[:, cut] = (value + got_z[u].astype(jnp.float32)).astype(jnp.bfloat16)
-
-    tok_swap(mine).wait_send()
-    gathers = [(tok, 0, mine), (tok, 1, theirs)]
-    for h in halves:
-        gathers.append((res, 2 + h, held_rows(MINE, h)))
-        gathers.append((res, 2 + SEQS_DEV + h, held_rows(THEIRS, h)))
-        res_swap(MINE, h).wait_send()
-        mix_swap(h).wait_send()
-    for gather in gathers:
-        wait_send(all_copies(*gather, "over"))
-        wait_send(all_copies(*gather, "pass"))
-    for o in (MINE, THEIRS):
-        for dx in range(n_x):
-            mix_core_copy(o, dx).wait_send()
-        for dx in range(1, n_x):
-            for h in halves:
-                mix_x_copy(o, h, dx).wait_send()
-    for u in range(n_out):
-        for dx in range(n_x):
-            core_copy(u, dx).wait_send()
-        for dx in range(1, n_x):
-            x_copy(u, dx).wait_send()
-        back(u).wait_send()
-
-    for s in order:
-        for d in range(1, n_fs):
-            wait_send(z_sends(s, d))
-            wait_send(y_copies(s, d, g))
+        with jax.named_scope("over_z_last"):
+            over_z(u)
+    with jax.named_scope("final"):
+        for u in range(n_out):
+            cut = slice(u * LANES, (u + 1) * LANES)
+            value = res[k, mine, cut].astype(jnp.float32) + place_sum(u, 1)
+            back(u).wait_recv()
+            out[:, cut] = (value + got_z[u].astype(jnp.float32)).astype(jnp.bfloat16)
+
+    with jax.named_scope("drain"):
+        for i, view in enumerate(all_sums(n_from)):
+            to_y(view, view, y_send.at[i], y_recv.at[0]).wait_send()
+
+        @pl.when(at_end)
+        def _():
+            for i, view in enumerate(all_sums(n_from - 1)):
+                to_fs(view, view, z_send.at[i], z_recv.at[0, 0], pair).wait_send()
+
+        @pl.when(jnp.logical_not(at_end))
+        def _():
+            for i, view in enumerate(all_sums(n_from)):
+                to_fs(view, view, z_send.at[i], z_recv.at[0, 0], pair).wait_send()
+            for i, view in enumerate(all_sums(1)):
+                to_fs(view, view, f_send.at[i], z_recv.at[0, 0], pair).wait_send()
+
+        for i, buffer in enumerate((tok, res)):
+            view = buffer.at[pl.ds(0, n_tp - 1)]
+            to_tp(view, view, all_send.at[i], all_recv.at[0, 0], core).wait_send()
+        view = part_mix.at[:, pl.ds(0, n_x)]
+        to_tp(view, view, mix_core_send.at[0], all_recv.at[0, 0], core).wait_send()
+        to_tp(mix_x_sum, mix_x_sum, mix_x_send.at[0], all_recv.at[0, 0], core).wait_send()
+        view = part_ffn.at[:, :, pl.ds(0, n_x)]
+        to_tp(view, view, core_send.at[0], all_recv.at[0, 0], core).wait_send()
+        to_tp(sum_x, sum_x, x_send.at[0], all_recv.at[0, 0], core).wait_send()
+        view = tok.at[pl.ds(0, 2)]
+        to_pair(0, view, view).wait_send()
 
 
 def fused(n_fs, n_tp, *args):
@@ -684,6 +786,7 @@
     width = n_fs * shard
     args = list(args)
     args[1], args[7] = args[1].reshape(1, -1), args[7].reshape(1, -1)
+    args[10] = args[10].transpose(1, 0, 2)
     in_vmem = {1, 5, 7, 10, 11}
     n_x = n_tp // 2
     length = rows // SEQS_DEV
@@ -711,32 +814,33 @@
             held(2 * rows, units),
             held(2, n_tp, rows, cols),
             held(2, n_x, rows, cols),
-            held(2, SEQS_DEV, n_x, length, cols),
-            held(2, SEQS_DEV, n_x, length, cols),
+            held(2, SEQS_DEV, n_x - 1, length, cols),
+            held(2, SEQS_DEV, n_x - 1, length, cols),
             held(SEQS_DEV, length, cols),
             held(SEQS_DEV, length, cols),
             held(n_out, 2, n_tp, rows, LANES),
             held(n_out, 2, n_x, rows, LANES),
-            held(n_out, n_x, 2, rows, LANES),
-            held(n_out, n_x, 2, rows, LANES),
+            held(n_out, n_x - 1, 2, rows, LANES),
+            held(n_out, n_x - 1, 2, rows, LANES),
             held(n_out, rows, LANES),
             held(n_out, rows, LANES),
-            dma((4 + 2 * n_in + n_out, n_fs)),
-            dma((4 + 2 * n_in + n_out, n_fs)),
+            dma((4,)),
             dma((2 + n_in + n_out, n_fs)),
-            dma((2 + n_in + n_out, n_fs)),
-            dma((5 + 2 * n_in + n_out,)),
-            dma((2 + 2 * SEQS_DEV, 2, n_x)),
-            dma((2 + 2 * SEQS_DEV, 2, n_x)),
+            dma((4,)),
+            dma((4,)),
+            dma((2 + n_in + n_out,)),
+            dma((5,)),
+            dma((2,)),
+            dma((2 + 2 * SEQS_DEV, 2 * n_x - 1)),
+            dma((1,)),
             dma((2, n_x)),
-            dma((2, n_x)),
-            dma((2, SEQS_DEV, n_x)),
-            dma((2, SEQS_DEV, n_x)),
+            dma((1,)),
+            dma((2, SEQS_DEV, n_x - 1)),
+            dma((1,)),
             dma((n_out, n_x)),
-            dma((n_out, n_x)),
-            dma((n_out, n_x)),
-            dma((n_out, n_x)),
-            dma((1 + 2 * SEQS_DEV + n_out,)),
+            dma((1,)),
+            dma((n_out, n_x - 1)),
+            dma((1,)),
             dma((1 + 2 * SEQS_DEV + n_out,)),
         ],
         compiler_params=pltpu.CompilerParams(
@@ -748,7 +852,7 @@
 def solution(mesh):
     n_fs, n_tp = mesh.shape["fs"], mesh.shape["tp"]
     body = functools.partial(fused, n_fs, n_tp)
-    if n_fs > 8 or n_fs != n_tp or n_fs % 2 or mesh.shape["grp"] != 2:
+    if n_fs != 4 or n_tp != 4 or mesh.shape["grp"] != 2:
         body = on_device
     placed = (
         P(("grp", "fs"), "tp"),

time: 163 us -> 143 us (0.88)
  Pallas kernels: 159 us -> 141 us
    pallas_call x1, Pallas kernels: 159 us -> 141 us  [fused(): pl.pallas_call(functools.partial(layer_kernel, n_fs, n_tp), out_shape=jax...]
where the time goes in v2:
time: 143 us; the launch traced here: 142 us
  Pallas kernels  141 us (99%)
  local copies, waits for them, and re-layouts  1.77 us (1%)
    pallas_call x1, Pallas kernels, fused(): pl.pallas_call(functools.partial(layer_kernel, n_fs, n_tp), out_shape=jax...  141 us

profile of v2, /device:TPU:0, one launch (start us, length us, event | category | flops | bytes accessed | tf_op | source)
XLA Modules:
  0.0 142.5 jit_solution(6193144447554587519)
XLA Ops:
  0.0 140.7 %shard_map.127 = bf16[384,512]{1,0:T(8,128)(2,1)} custom-call(bf16[384,512]{1,0:T(8,128)(2,1)} %tokens.1, f32[1,2048]{1,0:T(1,128)} %bitcast.4, bf16[512,256]{1,0:T(8,128)(2,1)} %w_signal.1, bf16[512,256]{1,0:T(8,128)(2,1)} %w_outer_gate.1, bf16[512,256]{1,0:T(8,128)(2,1)} %w_inner_gate.1, f32[3,256]{1,0:T(4,128)} %mix_taps.1, bf16[256,512]{1,0:T(8,128)(2,1)} %w_mix_out.1, ...), custom_call_target="tpu_custom_call" | custom-call | tf_op jit(solution)/shard_map/pallas_call | solution.py:798
  140.7 1.8 %copy.15 = bf16[384,512]{1,0:T(8,128)(2,1)} copy(bf16[384,512]{1,0:T(8,128)(2,1)} %shard_map.127) | data formatting | bytes 786432

commit v3 on v2

--- a/solution.py
+++ b/solution.py
@@ -108,6 +108,14 @@
         + shifted(values, 1, length) * taps[1]
         + values * taps[2]
     )
+
+
+END, INNER = 0, 1
+
+
+def tiles_of(n_tiles, role):
+    at_end = 2 * n_tiles // 5
+    return at_end if role == END else n_tiles - at_end
 
 
 def layer_kernel(
@@ -171,8 +179,9 @@
     length = rows // SEQS_DEV
     shard, chans = w_signal.shape
     half, unit_chans = shard // 2, chans // 2
-    units = w_gate.shape[1] // 2
-    n_in, n_out = units // LANES, shard // LANES
+    n_tiles, n_out = w_gate.shape[1] // LANES, shard // LANES
+    tiles = {END: tiles_of(n_tiles, END), INNER: tiles_of(n_tiles, INNER)}
+    base = {END: 0, INNER: tiles[END]}
     n_x = n_tp // 2
     x, c = k // 2, lax.rem(k, 2)
     core = k + 1 - 2 * c
@@ -193,28 +202,35 @@
         return slice(h * length, (h + 1) * length)
 
     mix = ("mix", 0)
-    order = [mix, *(("in", t) for t in range(n_in)), *(("out", u) for u in range(n_out))]
+    n_in = tiles[INNER]
+    ins = [("in", t) for t in range(n_in)]
+    outs = [("out", u) for u in range(n_out)]
+
+    def by_role(body):
+        pl.when(at_end)(functools.partial(body, END))
+        pl.when(jnp.logical_not(at_end))(functools.partial(body, INNER))
+
 
     def other(d):
         return lax.rem(j + inward * d, n_fs)
 
-    def sources(stage, q, side):
+    def sources(stage, role, side):
         kind, i = stage
         at_rows = pl.ds(pl.multiple_of(side * half, half), half)
         if kind == "mix":
-            lanes = pl.ds(pl.multiple_of(q * unit_chans, unit_chans), unit_chans)
+            lanes = pl.ds(role * unit_chans, unit_chans)
             tall = unit_chans // 2
-            at = pl.ds(pl.multiple_of((q * 2 + side) * tall, tall), tall)
+            at = pl.ds(pl.multiple_of(role * unit_chans + side * tall, tall), tall)
             refs = [ref.at[at_rows, lanes] for ref in (w_signal, w_outer_gate, w_inner_gate)]
             return [*refs, w_mix_out.at[at, :]]
         if kind == "in":
-            lanes = pl.ds(pl.multiple_of(q * units + i * LANES, LANES), LANES)
+            lanes = pl.ds((base[role] + i) * LANES, LANES)
             return [w_gate.at[at_rows, lanes], w_value.at[at_rows, lanes]]
-        tall = units // 2
-        at = pl.ds(pl.multiple_of((q * 2 + side) * tall, tall), tall)
+        tall = tiles[role] * LANES // 2
+        at = pl.ds(pl.multiple_of(base[role] * LANES + side * tall, LANES), tall)
         return [w_down.at[at, pl.ds(i * LANES, LANES)]]
 
-    def places(stage, source, side, whole):
+    def places(stage, role, source, side, whole):
         kind, i = stage
         at_rows = pl.ds(pl.multiple_of((source * 2 + side) * half, half), half)
         if kind == "mix":
@@ -229,8 +245,8 @@
             if whole:
                 return [ffn_in.at[i, at_rows, :]]
             return [ffn_in.at[i, at_rows, pl.ds(b * LANES, LANES)] for b in (0, 1)]
-        tall = units // 2
-        at = pl.ds(pl.multiple_of(side * tall, tall), tall)
+        tall = tiles[role] * LANES // 2
+        at = pl.ds(pl.multiple_of(side * tall, LANES), tall)
         lanes = pl.ds(pl.multiple_of(source * LANES, LANES), LANES)
         return [ffn_out.at[i, at, lanes]]
 
@@ -254,28 +270,32 @@
             device_id_type=MESH,
         )
 
-    def z_sends(s, d):
+    def role_of(role, d):
+        return INNER if d < n_fs - 1 - role else END
+
+    def z_sends(s, role, d):
         to = other(d)
-        pairs = zip(sources(s, lax.rem(to, 2), g), places(s, j, g, False))
+        there = role_of(role, d)
+        pairs = zip(sources(s, there, g), places(s, there, j, g, False))
         copies = []
         for i, (src, dst) in enumerate(pairs):
             wide = i // 3 if s[0] == "mix" else 0
-            sems = z_send.at[group(s, wide)], z_recv.at[slot(s, wide), j]
+            sems = z_send.at[group(s, wide), d - 1], z_recv.at[slot(s, wide), j]
             copies.append(to_fs(src, dst, *sems, to))
         return copies
 
-    def z_takes(s, d):
+    def z_takes(s, role, d):
         source = other(d)
         return [
-            to_fs(view, view, z_send.at[group(s, i)], z_recv.at[slot(s, i), source], source)
-            for i, view in enumerate(places(s, source, g, True))
+            to_fs(view, view, z_send.at[group(s, i), 0], z_recv.at[slot(s, i), source], source)
+            for i, view in enumerate(places(s, role, source, g, True))
         ]
 
     def z_forwards(s):
-        source = other(n_fs - 1)
+        source = other(last)
         return [
-            to_fs(view, view, f_send.at[group(s, i)], z_recv.at[slot(s, i), source], other(n_fs - 2))
-            for i, view in enumerate(places(s, source, g, True))
+            to_fs(view, view, f_send.at[group(s, i)], z_recv.at[slot(s, i), source], other(1))
+            for i, view in enumerate(places(s, INNER, source, g, True))
         ]
 
     def to_y(src, dst, send_sem, recv_sem):
@@ -288,29 +308,28 @@
             device_id_type=MESH,
         )
 
-    def y_copies(s, d):
+    def y_copies(s, role, d):
         return [
             to_y(view, view, y_send.at[group(s, i)], y_recv.at[slot(s, i)])
-            for i, view in enumerate(places(s, other(d), g, True))
+            for i, view in enumerate(places(s, role, other(d), g, True))
         ]
 
     n_from = n_fs - 1
 
-    def sums(stage):
+    def sums(stage, role, count):
         kind, i = stage
         if kind == "mix":
-            some = mix_out.at[pl.ds(0, n_from), pl.ds(0, unit_chans // 2), :]
-            return [mix_in.at[pl.ds(0, n_from * half), :], some]
+            some = mix_out.at[pl.ds(0, count), pl.ds(0, unit_chans // 2), :]
+            return [mix_in.at[pl.ds(0, count * half), :], some]
         if kind == "in":
-            return [ffn_in.at[i, pl.ds(0, n_from * half), :]]
-        return [ffn_out.at[i, pl.ds(0, units // 2), pl.ds(0, n_from * LANES)]]
-
-    def all_sums(count):
+            return [ffn_in.at[i, pl.ds(0, count * half), :]]
+        return [ffn_out.at[i, pl.ds(0, tiles[role] * LANES // 2), pl.ds(0, count * LANES)]]
+
+    def all_sums(role, count):
         return [
-            mix_in.at[pl.ds(0, count * half), :],
-            mix_out.at[pl.ds(0, count), pl.ds(0, unit_chans // 2), :],
-            ffn_in.at[:, pl.ds(0, count * half), :],
-            ffn_out.at[:, pl.ds(0, units // 2), pl.ds(0, count * LANES)],
+            *sums(mix, role, count),
+            *sums(("in", pl.ds(0, tiles[role])), role, count),
+            *sums(("out", pl.ds(0, n_out)), role, count),
         ]
 
     def start(copies):
@@ -325,35 +344,32 @@
         for copy in copies:
             copy.wait_send()
 
-    def send(s, ds):
+    def send(s, role, ds):
         for d in ds:
-            start(z_sends(s, d))
-
-    straight, last = range(1, n_fs - 1), n_fs - 1
-
-    def relay(s, d):
-        wait_recv(z_takes(s, d))
-        start(y_copies(s, d))
-
-    def relay_all(s, following=()):
-        relay(s, 1)
-
-        @pl.when(at_end)
-        def _():
-            for d in range(2, n_fs):
-                relay(s, d)
-
-        @pl.when(jnp.logical_not(at_end))
-        def _():
-            relay(s, last)
-            start(z_forwards(s))
-            for later in following:
-                send(later, straight)
-            for d in range(2, n_fs - 1):
-                relay(s, d)
-
-    def arrived(s):
-        for i, view in enumerate(sums(s)):
+            if s[0] != "in" or s[1] < tiles[role_of(role, d)]:
+                start(z_sends(s, role, d))
+
+    last = n_fs - 1
+
+    def relay(s, role, d):
+        wait_recv(z_takes(s, role, d))
+        start(y_copies(s, role, d))
+
+    def ahead(s):
+        relay(s, INNER, last)
+        start(z_forwards(s))
+
+    def relay_all(s, role):
+        if s[0] == "in" and s[1] >= tiles[role]:
+            return
+        for d in (1, 2, last) if role == END else (1, 2):
+            relay(s, role, d)
+
+    def relay_both(s):
+        by_role(lambda role: relay_all(s, role))
+
+    def arrived(s, role):
+        for i, view in enumerate(sums(s, role, n_from)):
             to_y(view, view, y_send.at[group(s, i)], y_recv.at[slot(s, i)]).wait_recv()
 
     def to_tp(src, dst, send_sem, recv_sem, to):
@@ -367,7 +383,7 @@
         )
 
     def all_copies(buffer, i, at, kind):
-        sent = all_send.at[0 if i < 2 else 1]
+        sent = all_send.at[0 if i <= SEQS_DEV else 1]
         copies = []
         for dx in range(n_x):
             there = lax.rem(x + dx, n_x)
@@ -390,7 +406,7 @@
         passed = all_copies(buffer, i, at, "pass")
         for dx in range(1, n_x):
             view = buffer.at[lax.rem(x + n_x - dx, n_x) * 2 + c, at]
-            sent = all_send.at[0 if i < 2 else 1]
+            sent = all_send.at[0 if i <= SEQS_DEV else 1]
             to_tp(view, view, sent, all_recv.at[i, dx - 1], core).wait_recv()
             passed[dx].start()
 
@@ -410,18 +426,19 @@
     halves = range(SEQS_DEV)
     mine, theirs = held_rows(MINE), held_rows(THEIRS)
 
-    def tok_swap(at):
-        return to_pair(0, tok.at[k, at], tok.at[k, at])
+    def tok_swap(o, h):
+        view = tok.at[k, held_rows(o, h)]
+        return to_pair(h, view, view)
 
     def res_swap(o, h):
         view = res.at[k, held_rows(o, h)]
-        return to_pair(1 + h, view, view)
+        return to_pair(SEQS_DEV + h, view, view)
 
     def mix_swap(h):
-        return to_pair(1 + SEQS_DEV + h, mix_z_sum.at[h], mix_z_got.at[h])
+        return to_pair(2 * SEQS_DEV + h, mix_z_sum.at[h], mix_z_got.at[h])
 
     def back(u):
-        return to_pair(1 + 2 * SEQS_DEV + u, sum_z.at[u], got_z.at[u])
+        return to_pair(3 * SEQS_DEV + u, sum_z.at[u], got_z.at[u])
 
     barrier = pltpu.get_barrier_semaphore()
     for d in range(1, n_fs):
@@ -435,8 +452,8 @@
     first = pltpu.make_async_copy(tokens, tok.at[k, mine], load_sem.at[4])
     own_rows = pl.ds(pl.multiple_of(j * shard, shard), shard)
     own_lanes = pl.ds(pl.multiple_of(j * LANES, LANES), LANES)
-    at_chans = pl.ds(pl.multiple_of(p * unit_chans, unit_chans), unit_chans)
-    at_units = pl.ds(pl.multiple_of(p * units, units), units)
+    inner_role = jnp.where(at_end, END, INNER)
+    at_chans = pl.ds(pl.multiple_of(inner_role * unit_chans, unit_chans), unit_chans)
 
     def load(i, src, dst):
         pltpu.make_async_copy(src, dst, load_sem.at[i]).start()
@@ -445,40 +462,48 @@
     for i, ref in enumerate((w_signal, w_outer_gate, w_inner_gate)):
         load(0, ref.at[:, at_chans], mix_in.at[own_rows, pl.ds(i * unit_chans, unit_chans)])
     load(1, w_mix_out.at[at_chans, :], mix_out.at[j])
-    for t in range(n_in):
-        lanes = pl.ds(pl.multiple_of(p * units + t * LANES, LANES), LANES)
-        for i, ref in enumerate((w_gate, w_value)):
-            load(2, ref.at[:, lanes], ffn_in.at[t, own_rows, pl.ds(i * LANES, LANES)])
-    for u in range(n_out):
-        load(3, w_down.at[at_units, pl.ds(u * LANES, LANES)], ffn_out.at[u, :, own_lanes])
-    loaded = [
-        mix_in.at[own_rows, :],
-        mix_out.at[j],
-        ffn_in.at[:, own_rows, :],
-        ffn_out.at[:, :, own_lanes],
-    ]
+    def load_ffn(role):
+        for t in range(tiles[role]):
+            for i, src in enumerate((w_gate, w_value)):
+                lanes = pl.ds((base[role] + t) * LANES, LANES)
+                load(2, src.at[:, lanes], ffn_in.at[t, own_rows, pl.ds(i * LANES, LANES)])
+        tall = tiles[role] * LANES
+        for u in range(n_out):
+            src = w_down.at[pl.ds(base[role] * LANES, tall), pl.ds(u * LANES, LANES)]
+            load(3, src, ffn_out.at[u, pl.ds(0, tall), own_lanes])
+
+    def wait_loads(role):
+        views = [
+            mix_in.at[own_rows, :],
+            mix_out.at[j],
+            ffn_in.at[pl.ds(0, tiles[role]), own_rows, :],
+            ffn_out.at[:, pl.ds(0, tiles[role] * LANES), own_lanes],
+        ]
+        for i, view in enumerate(views):
+            pltpu.make_async_copy(view, view, load_sem.at[i]).wait()
+
     with jax.named_scope("barrier"):
         first.wait()
         pl.semaphore_wait(barrier, n_fs - 1 + 1 + n_tp - 1)
 
-    send(mix, (1,))
-
-    @pl.when(at_end)
-    def _():
-        tok_swap(mine).start()
+    def begin(role):
+        send(mix, role, (1, last) if role == END else (last, 1))
+        tok_swap(MINE, 0).start()
         all_begin(tok, 0, mine)
-        send(mix, range(2, n_fs - 1))
-
-    @pl.when(jnp.logical_not(at_end))
-    def _():
-        send(mix, (last,))
-        tok_swap(mine).start()
-        all_begin(tok, 0, mine)
-        send(mix, range(2, n_fs - 1))
-
+        if role == INNER:
+            send(mix, role, (2,))
+        for h in halves[1:]:
+            tok_swap(MINE, h).start()
+        if role == END:
+            for s in ins:
+                send(s, role, (1,))
+            for s in ins[:2]:
+                send(s, role, (last,))
+        load_ffn(role)
+
+    by_role(begin)
     with jax.named_scope("loads"):
-        for i, view in enumerate(loaded):
-            pltpu.make_async_copy(view, view, load_sem.at[i]).wait()
+        by_role(wait_loads)
 
     def norm(buffer, at, gain):
         count = at.size
@@ -494,50 +519,63 @@
 
     with jax.named_scope("tok_mid"):
         all_middle(tok, 0, mine)
-    with jax.named_scope("relay_mix1"):
-        relay(mix, 1)
-
-    @pl.when(at_end)
-    def _():
-        with jax.named_scope("relay_mix2"):
-            relay(mix, 2)
-
-    @pl.when(jnp.logical_not(at_end))
-    def _():
-        with jax.named_scope("relay_mix2"):
-            relay(mix, last)
-            start(z_forwards(mix))
-
-    with jax.named_scope("norm_mine"):
-        all_end(tok, 0, mine)
-        norm(tok, mine, mix_gain)
-    with jax.named_scope("tok_swap"):
-        tok_swap(theirs).wait_recv()
-        all_begin(tok, 1, theirs)
-
-    @pl.when(at_end)
-    def _():
-        with jax.named_scope("relay_mix3"):
-            relay(mix, last)
-        for s in order[1:4]:
-            send(s, straight)
-
-    @pl.when(jnp.logical_not(at_end))
-    def _():
-        with jax.named_scope("relay_mix3"):
-            relay(mix, 2)
-        for s in order[1:3]:
-            send(s, straight)
-        for s in order[1:4]:
-            send(s, (last,))
-
-    with jax.named_scope("tok_theirs"):
-        all_middle(tok, 1, theirs)
+    def take_tok(h):
+        with jax.named_scope("tok_swap"):
+            tok_swap(THEIRS, h).wait_recv()
+            all_begin(tok, 1 + h, held_rows(THEIRS, h))
+
+    def pass_tok(h):
+        with jax.named_scope("tok_theirs"):
+            all_middle(tok, 1 + h, held_rows(THEIRS, h))
+
+    def early(role):
+        if role == END:
+            with jax.named_scope("relay_mix"):
+                relay(mix, role, 1)
+            take_tok(0)
+            with jax.named_scope("norm_mine"):
+                all_end(tok, 0, mine)
+                norm(tok, mine, mix_gain)
+            with jax.named_scope("relay_mix"):
+                relay(mix, role, 2)
+            pass_tok(0)
+            for h in halves[1:]:
+                take_tok(h)
+            with jax.named_scope("relay_mix"):
+                relay(mix, role, last)
+            for h in halves[1:]:
+                pass_tok(h)
+            return
+        with jax.named_scope("relay_mix"):
+            relay(mix, role, 1)
+        with jax.named_scope("relay_mix"):
+            ahead(mix)
+        send(ins[0], role, (1, 2))
+        take_tok(0)
+        with jax.named_scope("norm_mine"):
+            all_end(tok, 0, mine)
+            norm(tok, mine, mix_gain)
+        for h in halves[1:]:
+            take_tok(h)
+        pass_tok(0)
+        with jax.named_scope("relay_mix"):
+            relay(mix, role, 2)
+        for s in ins[:3]:
+            send(s, role, (last,))
+        with jax.named_scope("ahead0"):
+            ahead(ins[0])
+            send(ins[1], role, (1, 2))
+        for h in halves[1:]:
+            pass_tok(h)
+
+    by_role(early)
     with jax.named_scope("norm_theirs"):
-        all_end(tok, 1, theirs)
+        for h in halves:
+            all_end(tok, 1 + h, held_rows(THEIRS, h))
         norm(tok, theirs, mix_gain)
     with jax.named_scope("arrived_mix"):
-        arrived(mix)
+        arrived(mix, INNER)
+
     taps = [mix_taps[i : i + 1, at_chans] for i in range(3)]
 
     def mix_core_copy(o, dx):
@@ -593,8 +631,17 @@
                     mix_x_sum[o, h, dx - 1] = mix_chip_sum(o, h, dx).astype(jnp.bfloat16)
                     mix_x_copy(o, h, dx).start()
             mix_core_copy(o, 0).wait_recv()
-    with jax.named_scope("relay_in0"):
-        relay_all(order[1], order[3:4])
+    def between(role):
+        if role == INNER:
+            with jax.named_scope("ahead1"):
+                for at in (1, 2):
+                    ahead(ins[at])
+                    send(ins[at + 1], role, (1, 2))
+        with jax.named_scope("relay_in0"):
+            relay_all(ins[0], role)
+
+    by_role(between)
+
     with jax.named_scope("mix_x_theirs"):
         for h in halves:
             for dx in range(1, n_x):
@@ -602,8 +649,21 @@
             mix_z_sum[h] = mix_place_sum(THEIRS, h).astype(jnp.bfloat16)
             mix_swap(h).start()
 
-    with jax.named_scope("relay_in1"):
-        relay_all(order[2], order[4:5])
+    def second(role):
+        if role == END:
+            send(ins[2], role, (last,))
+            for s in outs[:2]:
+                send(s, role, (1,))
+        else:
+            with jax.named_scope("ahead3"):
+                for at in range(3, n_in):
+                    ahead(ins[at])
+                    if at + 1 < n_in:
+                        send(ins[at + 1], role, (1, 2))
+        with jax.named_scope("relay_in1"):
+            relay_all(ins[1], role)
+
+    by_role(second)
     with jax.named_scope("mix_mine"):
         for h in halves:
             for dx in range(1, n_x):
@@ -613,46 +673,59 @@
             at = held_rows(MINE, h)
             res[k, at, :] = (tok[k, at, :].astype(jnp.float32) + mixer).astype(jnp.bfloat16)
             res_swap(MINE, h).start()
-            all_begin(res, 2 + h, at)
-
-    @pl.when(at_end)
-    def _():
-        for s in order[4:]:
-            send(s, straight)
-
+            all_begin(res, 1 + SEQS_DEV + h, at)
+
+    def third(role):
+        for s in outs[2:] if role == END else ():
+            send(s, role, (1,))
+        for s in ins[3:]:
+            send(s, role, (last,))
+        for s in outs:
+            send(s, role, (2, last) if role == END else (1, 2, last))
+        with jax.named_scope("relay_in2"):
+            relay_all(ins[2], role)
+
+    by_role(third)
+    with jax.named_scope("res_mid"):
+        for h in halves:
+            all_middle(res, 1 + SEQS_DEV + h, held_rows(MINE, h))
     @pl.when(jnp.logical_not(at_end))
     def _():
-        for s in order[4:]:
-            send(s, (last,))
-
-
-    with jax.named_scope("relay_in2"):
-        relay_all(order[3], order[5:6])
-    with jax.named_scope("res_mid"):
-        for h in halves:
-            all_middle(res, 2 + h, held_rows(MINE, h))
+        with jax.named_scope("relay_in3"):
+            relay_all(ins[3], INNER)
+
     with jax.named_scope("res_swap"):
         for h in halves:
             res_swap(THEIRS, h).wait_recv()
-            all_begin(res, 2 + SEQS_DEV + h, held_rows(THEIRS, h))
+            all_begin(res, 1 + 2 * SEQS_DEV + h, held_rows(THEIRS, h))
+    @pl.when(at_end)
+    def _():
+        with jax.named_scope("relay_in3"):
+            relay_all(ins[3], END)
+
+    @pl.when(jnp.logical_not(at_end))
+    def _():
+        for s in outs[:2]:
+            relay(s, INNER, last)
+
     with jax.named_scope("res_norm"):
         for h in halves:
-            all_end(res, 2 + h, held_rows(MINE, h))
+            all_end(res, 1 + SEQS_DEV + h, held_rows(MINE, h))
             norm(res, held_rows(MINE, h), ffn_gain)
     with jax.named_scope("res_mid2"):
         for h in halves:
-            all_middle(res, 2 + SEQS_DEV + h, held_rows(THEIRS, h))
-    with jax.named_scope("relay_in3"):
-        relay_all(order[4], order[6:7])
+            all_middle(res, 1 + 2 * SEQS_DEV + h, held_rows(THEIRS, h))
     with jax.named_scope("res_norm2"):
         for h in halves:
-            all_end(res, 2 + SEQS_DEV + h, held_rows(THEIRS, h))
+            all_end(res, 1 + 2 * SEQS_DEV + h, held_rows(THEIRS, h))
             norm(res, held_rows(THEIRS, h), ffn_gain)
+
+    first_tile = jnp.where(at_end, base[END], base[INNER])
 
     def feed(t):
         with jax.named_scope("in_wait"):
-            arrived(("in", t))
-        cut = pl.ds(pl.multiple_of(p * units + t * LANES, LANES), LANES)
+            arrived(("in", t), INNER)
+        cut = pl.ds(pl.multiple_of((first_tile + t) * LANES, LANES), LANES)
         both = jnp.dot(normed[...], ffn_in[t], preferred_element_type=jnp.float32)
         both = both.astype(jnp.bfloat16).astype(jnp.float32)
         gate_taps, value_taps = ([up_taps[i, b : b + 1, cut] for i in range(3)] for b in (0, 1))
@@ -661,33 +734,45 @@
         unit = (gate / (1.0 + jnp.exp(-gate)) * value).astype(jnp.bfloat16)
         hidden[:, pl.ds(pl.multiple_of(t * LANES, LANES), LANES)] = unit
 
-    beside = {2: 5, 3: 6, 4: 7}
-
-    @pl.loop(0, n_in)
+    beside = {
+        (INNER, 1): (ins[4],),
+        (INNER, 2): outs[2:],
+        (INNER, 3): (ins[5],),
+        (INNER, 5): (outs[0],),
+        (END, 2): (outs[0],),
+        (END, 3): (outs[1],),
+    }
+
+    @pl.loop(0, jnp.where(at_end, tiles[END], tiles[INNER]))
     def _(t):
-        for at, index in beside.items():
-
-            @pl.when(t == at)
+        for (role, at), stages in beside.items():
+            here = at_end if role == END else jnp.logical_not(at_end)
+
+            @pl.when(here & (t == at))
             def _():
-                with jax.named_scope("relay_out"):
-                    relay_all(order[index], order[index + 2 : index + 3])
+                with jax.named_scope("relay_beside"):
+                    for stage in stages:
+                        if len(stages) > 1:
+                            relay(stage, role, last)
+                        else:
+                            relay_all(stage, role)
 
         feed(t)
 
-    def core_copy(u, dx):
+    def core_copy(u, o, dx):
         there = lax.rem(x + dx, n_x)
         return to_tp(
-            part_ffn.at[u, :, there * 2 + 1 - c],
-            got_core.at[u, :, there],
+            part_ffn.at[u, o, there * 2 + 1 - c],
+            got_core.at[u, o, there],
             core_send.at[0],
-            core_recv.at[u, dx],
+            core_recv.at[u, o, dx],
             core,
         )
 
-    def x_copy(u, dx):
+    def x_copy(u, o, dx):
         to = lax.rem(x + dx, n_x) * 2 + c
-        sems = x_send.at[0], x_recv.at[u, dx - 1]
-        return to_tp(sum_x.at[u, dx - 1], got_x.at[u, dx - 1], *sems, to)
+        sems = x_send.at[0], x_recv.at[u, o, dx - 1]
+        return to_tp(sum_x.at[u, o, dx - 1], got_x.at[u, o, dx - 1], *sems, to)
 
     def chip_sum(u, o, dx):
         there = lax.rem(x + dx, n_x)
@@ -697,73 +782,75 @@
     def place_sum(u, o):
         value = chip_sum(u, o, 0)
         for dx in range(1, n_x):
-            value = value + got_x[u, dx - 1, o].astype(jnp.float32)
+            value = value + got_x[u, o, dx - 1].astype(jnp.float32)
         return value
 
-    def down(u):
+    def down(u, role):
         with jax.named_scope("out_wait"):
-            arrived(("out", u))
-        for o, at in enumerate((theirs, mine)):
-            terms = jnp.dot(hidden[at, :], ffn_out[u], preferred_element_type=jnp.float32)
+            arrived(("out", u), role)
+        deep = pl.ds(0, tiles[role] * LANES)
+        for o, at in ((THEIRS, theirs), (MINE, mine)):
+            left, right = hidden[at, deep], ffn_out[u, deep, :]
+            terms = jnp.dot(left, right, preferred_element_type=jnp.float32)
             for b in range(n_tp):
                 part_ffn[u, o, b] = terms[:, b * LANES : (b + 1) * LANES].astype(jnp.bfloat16)
-        for dx in (*range(1, n_x), 0):
-            core_copy(u, dx).start()
+            for dx in (*range(1, n_x), 0):
+                core_copy(u, o, dx).start()
 
     def over_x(u):
+        for o in (THEIRS, MINE):
+            for dx in range(1, n_x):
+                core_copy(u, o, dx).wait_recv()
+                sum_x[u, o, dx - 1] = chip_sum(u, o, dx).astype(jnp.bfloat16)
+                x_copy(u, o, dx).start()
+
+    def over_z(u):
+        core_copy(u, THEIRS, 0).wait_recv()
         for dx in range(1, n_x):
-            core_copy(u, dx).wait_recv()
-            for o in (0, 1):
-                sum_x[u, dx - 1, o] = chip_sum(u, o, dx).astype(jnp.bfloat16)
-            x_copy(u, dx).start()
-
-    def over_z(u):
-        core_copy(u, 0).wait_recv()
-        for dx in range(1, n_x):
-            x_copy(u, dx).wait_recv()
-        sum_z[u] = place_sum(u, 0).astype(jnp.bfloat16)
+            x_copy(u, THEIRS, dx).wait_recv()
+        sum_z[u] = place_sum(u, THEIRS).astype(jnp.bfloat16)
         back(u).start()
 
     for u in range(n_out):
-        if 8 + u < len(order):
-            with jax.named_scope("relay_out2"):
-                relay_all(order[8 + u], order[10 + u : 11 + u])
-        with jax.named_scope("down"):
-            down(u)
+        def step(role):
+            at = u + 1 + (role == END)
+            if at < n_out:
+                with jax.named_scope("relay_out"):
+                    relay_all(outs[at], role)
+            with jax.named_scope("down"):
+                down(u, role)
+
+        by_role(step)
+        with jax.named_scope("over_x"):
+            over_x(u)
         if u >= 1:
-            with jax.named_scope("over_x"):
-                over_x(u - 1)
-        if u >= 2:
             with jax.named_scope("over_z"):
-                over_z(u - 2)
-    with jax.named_scope("over_x_last"):
-        over_x(n_out - 1)
-    for u in range(max(n_out - 2, 0), n_out):
-        with jax.named_scope("over_z_last"):
-            over_z(u)
+                over_z(u - 1)
+    with jax.named_scope("over_z_last"):
+        over_z(n_out - 1)
     with jax.named_scope("final"):
         for u in range(n_out):
             cut = slice(u * LANES, (u + 1) * LANES)
-            value = res[k, mine, cut].astype(jnp.float32) + place_sum(u, 1)
+            core_copy(u, MINE, 0).wait_recv()
+            for dx in range(1, n_x):
+                x_copy(u, MINE, dx).wait_recv()
+            value = res[k, mine, cut].astype(jnp.float32) + place_sum(u, MINE)
             back(u).wait_recv()
             out[:, cut] = (value + got_z[u].astype(jnp.float32)).astype(jnp.bfloat16)
 
     with jax.named_scope("drain"):
-        for i, view in enumerate(all_sums(n_from)):
-            to_y(view, view, y_send.at[i], y_recv.at[0]).wait_send()
-
-        @pl.when(at_end)
-        def _():
-            for i, view in enumerate(all_sums(n_from - 1)):
-                to_fs(view, view, z_send.at[i], z_recv.at[0, 0], pair).wait_send()
-
-        @pl.when(jnp.logical_not(at_end))
-        def _():
-            for i, view in enumerate(all_sums(n_from)):
-                to_fs(view, view, z_send.at[i], z_recv.at[0, 0], pair).wait_send()
-            for i, view in enumerate(all_sums(1)):
-                to_fs(view, view, f_send.at[i], z_recv.at[0, 0], pair).wait_send()
-
+        def drain(role):
+            for i, view in enumerate(all_sums(role, n_from)):
+                to_y(view, view, y_send.at[i], y_recv.at[0]).wait_send()
+            for d in range(1, n_fs):
+                for i, view in enumerate(all_sums(role_of(role, d), 1)):
+                    if (role, d) != (END, 2) or i == 3:
+                        to_fs(view, view, z_send.at[i, d - 1], z_recv.at[0, 0], pair).wait_send()
+            if role == INNER:
+                for i, view in enumerate(all_sums(role, 1)[:3]):
+                    to_fs(view, view, f_send.at[i], z_recv.at[0, 0], pair).wait_send()
+
+        by_role(drain)
         for i, buffer in enumerate((tok, res)):
             view = buffer.at[pl.ds(0, n_tp - 1)]
             to_tp(view, view, all_send.at[i], all_recv.at[0, 0], core).wait_send()
@@ -781,8 +868,8 @@
     tokens, w_signal, w_gate = args[0], args[2], args[8]
     rows, cols = tokens.shape
     shard, chans = w_signal.shape
-    units = w_gate.shape[1] // 2
-    n_in, n_out = units // LANES, shard // LANES
+    n_in, n_out = tiles_of(w_gate.shape[1] // LANES, INNER), shard // LANES
+    units = n_in * LANES
     width = n_fs * shard
     args = list(args)
     args[1], args[7] = args[1].reshape(1, -1), args[7].reshape(1, -1)
@@ -820,28 +907,28 @@
             held(SEQS_DEV, length, cols),
             held(n_out, 2, n_tp, rows, LANES),
             held(n_out, 2, n_x, rows, LANES),
-            held(n_out, n_x - 1, 2, rows, LANES),
-            held(n_out, n_x - 1, 2, rows, LANES),
+            held(n_out, 2, n_x - 1, rows, LANES),
+            held(n_out, 2, n_x - 1, rows, LANES),
             held(n_out, rows, LANES),
             held(n_out, rows, LANES),
-            dma((4,)),
+            dma((4, n_fs - 1)),
             dma((2 + n_in + n_out, n_fs)),
             dma((4,)),
             dma((4,)),
             dma((2 + n_in + n_out,)),
             dma((5,)),
             dma((2,)),
-            dma((2 + 2 * SEQS_DEV, 2 * n_x - 1)),
+            dma((1 + 3 * SEQS_DEV, 2 * n_x - 1)),
             dma((1,)),
             dma((2, n_x)),
             dma((1,)),
             dma((2, SEQS_DEV, n_x - 1)),
             dma((1,)),
-            dma((n_out, n_x)),
+            dma((n_out, 2, n_x)),
             dma((1,)),
-            dma((n_out, n_x - 1)),
+            dma((n_out, 2, n_x - 1)),
             dma((1,)),
-            dma((1 + 2 * SEQS_DEV + n_out,)),
+            dma((3 * SEQS_DEV + n_out,)),
         ],
         compiler_params=pltpu.CompilerParams(
             collective_id=0, has_side_effects=True, vmem_limit_bytes=62 * 1024 * 1024

time: 143 us -> 136 us (0.951)
  Pallas kernels: 141 us -> 134 us
    pallas_call x1, Pallas kernels: 141 us -> 134 us  [fused(): pl.pallas_call(functools.partial(layer_kernel, n_fs, n_tp), out_shape=jax...]
where the time goes in v3:
time: 136 us
  Pallas kernels  134 us (99%)
  local copies, waits for them, and re-layouts  1.77 us (1%)
    pallas_call x1, Pallas kernels, fused(): pl.pallas_call(functools.partial(layer_kernel, n_fs, n_tp), out_shape=jax...  134 us

profile of v3, /device:TPU:0, one launch (start us, length us, event | category | flops | bytes accessed | tf_op | source)
XLA Modules:
  0.0 136.0 jit_solution(7282344319308199241)
XLA Ops:
  0.0 134.3 %shard_map.127 = bf16[384,512]{1,0:T(8,128)(2,1)} custom-call(bf16[384,512]{1,0:T(8,128)(2,1)} %tokens.1, f32[1,2048]{1,0:T(1,128)} %bitcast.4, bf16[512,256]{1,0:T(8,128)(2,1)} %w_signal.1, bf16[512,256]{1,0:T(8,128)(2,1)} %w_outer_gate.1, bf16[512,256]{1,0:T(8,128)(2,1)} %w_inner_gate.1, f32[3,256]{1,0:T(4,128)} %mix_taps.1, bf16[256,512]{1,0:T(8,128)(2,1)} %w_mix_out.1, ...), custom_call_target="tpu_custom_call" | custom-call | tf_op jit(solution)/shard_map/pallas_call | solution.py:885
  134.3 1.8 %copy.15 = bf16[384,512]{1,0:T(8,128)(2,1)} copy(bf16[384,512]{1,0:T(8,128)(2,1)} %shard_map.127) | data formatting | bytes 786432

commit v4 on v3

--- a/solution.py
+++ b/solution.py
@@ -155,6 +155,7 @@
     got_x,
     sum_z,
     got_z,
+    done,
     z_send,
     z_recv,
     f_send,
@@ -448,6 +449,9 @@
     for d in range(1, n_tp):
         to = lax.rem(k + d, n_tp)
         pl.semaphore_signal(barrier, inc=1, device_id={"tp": to}, device_id_type=MESH)
+    for dx in range(1, n_x):
+        far = {"tp": lax.rem(x + dx, n_x) * 2 + c, "fs": pair}
+        pl.semaphore_signal(barrier, inc=1, device_id=far, device_id_type=MESH)
 
     first = pltpu.make_async_copy(tokens, tok.at[k, mine], load_sem.at[4])
     own_rows = pl.ds(pl.multiple_of(j * shard, shard), shard)
@@ -484,7 +488,7 @@
 
     with jax.named_scope("barrier"):
         first.wait()
-        pl.semaphore_wait(barrier, n_fs - 1 + 1 + n_tp - 1)
+        pl.semaphore_wait(barrier, n_fs - 1 + 1 + n_tp - 1 + n_x - 1)
 
     def begin(role):
         send(mix, role, (1, last) if role == END else (last, 1))
@@ -676,12 +680,12 @@
             all_begin(res, 1 + SEQS_DEV + h, at)
 
     def third(role):
+        for s in ins[3:]:
+            send(s, role, (last,))
         for s in outs[2:] if role == END else ():
             send(s, role, (1,))
-        for s in ins[3:]:
-            send(s, role, (last,))
-        for s in outs:
-            send(s, role, (2, last) if role == END else (1, 2, last))
+        for s in outs if role == INNER else ():
+            send(s, role, (1, 2, last))
         with jax.named_scope("relay_in2"):
             relay_all(ins[2], role)
 
@@ -712,6 +716,12 @@
         for h in halves:
             all_end(res, 1 + SEQS_DEV + h, held_rows(MINE, h))
             norm(res, held_rows(MINE, h), ffn_gain)
+    def fourth(role):
+        if role == INNER:
+            with jax.named_scope("relay_in4"):
+                relay_all(ins[4], INNER)
+
+    by_role(fourth)
     with jax.named_scope("res_mid2"):
         for h in halves:
             all_middle(res, 1 + 2 * SEQS_DEV + h, held_rows(THEIRS, h))
@@ -734,30 +744,47 @@
         unit = (gate / (1.0 + jnp.exp(-gate)) * value).astype(jnp.bfloat16)
         hidden[:, pl.ds(pl.multiple_of(t * LANES, LANES), LANES)] = unit
 
+    paced = {0: outs[:1], 2: outs[1:2], 3: outs[2:3]}
     beside = {
-        (INNER, 1): (ins[4],),
-        (INNER, 2): outs[2:],
-        (INNER, 3): (ins[5],),
-        (INNER, 5): (outs[0],),
-        (END, 2): (outs[0],),
-        (END, 3): (outs[1],),
+        (INNER, 2): [(ins[5], 1), (ins[5], 2)],
+        (INNER, 3): [(outs[2], last), (outs[3], last)],
+        (INNER, 4): [(outs[0], 2), (outs[0], 1)],
+        (END, 1): [(stage, 1) for stage in outs],
+        (END, 3): [(outs[0], last), (outs[0], 2)],
+    }
+    after = {
+        (INNER, 0): [(outs[1], 2), (outs[1], 1)],
+        (INNER, 1): [(outs[2], 2), (outs[2], 1)],
+        (INNER, 2): [(outs[3], 2), (outs[3], 1)],
+        (END, 0): [(outs[1], last), (outs[1], 2)],
+        (END, 1): [(outs[2], last), (outs[2], 2)],
+        (END, 2): [(outs[3], last), (outs[3], 2)],
     }
 
     @pl.loop(0, jnp.where(at_end, tiles[END], tiles[INNER]))
     def _(t):
-        for (role, at), stages in beside.items():
+        for at, stages in paced.items():
+
+            @pl.when(at_end & (t == at))
+            def _():
+                for stage in stages:
+                    send(stage, END, (2, last))
+
+        for (role, at), relays in beside.items():
             here = at_end if role == END else jnp.logical_not(at_end)
 
             @pl.when(here & (t == at))
             def _():
-                with jax.named_scope("relay_beside"):
-                    for stage in stages:
-                        if len(stages) > 1:
-                            relay(stage, role, last)
-                        else:
-                            relay_all(stage, role)
+                for stage, d in relays:
+                    with jax.named_scope("relay_beside"):
+                        relay(stage, role, d)
 
         feed(t)
+
+    @pl.when(at_end)
+    def _():
+        for stage in outs[3:]:
+            send(stage, END, (2, last))
 
     def core_copy(u, o, dx):
         there = lax.rem(x + dx, n_x)
@@ -771,8 +798,15 @@
 
     def x_copy(u, o, dx):
         to = lax.rem(x + dx, n_x) * 2 + c
-        sems = x_send.at[0], x_recv.at[u, o, dx - 1]
-        return to_tp(sum_x.at[u, o, dx - 1], got_x.at[u, o, dx - 1], *sems, to)
+        straight = u == n_out - 1 and o == THEIRS
+        return pltpu.make_async_remote_copy(
+            src_ref=sum_x.at[u, o, dx - 1],
+            dst_ref=got_x.at[u, o, dx - 1],
+            send_sem=x_send.at[0],
+            recv_sem=x_recv.at[u, o, dx - 1],
+            device_id={"tp": to, "fs": pair} if straight else {"tp": to},
+            device_id_type=MESH,
+        )
 
     def chip_sum(u, o, dx):
         there = lax.rem(x + dx, n_x)
@@ -806,28 +840,37 @@
 
     def over_z(u):
         core_copy(u, THEIRS, 0).wait_recv()
-        for dx in range(1, n_x):
-            x_copy(u, THEIRS, dx).wait_recv()
-        sum_z[u] = place_sum(u, THEIRS).astype(jnp.bfloat16)
+        if u == n_out - 1:
+            value = chip_sum(u, THEIRS, 0)
+        else:
+            for dx in range(1, n_x):
+                x_copy(u, THEIRS, dx).wait_recv()
+            value = place_sum(u, THEIRS)
+        sum_z[u] = value.astype(jnp.bfloat16)
         back(u).start()
 
     for u in range(n_out):
+        if u >= 2:
+            with jax.named_scope("over_z"):
+                over_z(u - 2)
+
         def step(role):
-            at = u + 1 + (role == END)
-            if at < n_out:
+            for stage, d in after.get((role, u), ()):
                 with jax.named_scope("relay_out"):
-                    relay_all(outs[at], role)
+                    relay(stage, role, d)
             with jax.named_scope("down"):
                 down(u, role)
 
         by_role(step)
         with jax.named_scope("over_x"):
             over_x(u)
-        if u >= 1:
-            with jax.named_scope("over_z"):
-                over_z(u - 1)
-    with jax.named_scope("over_z_last"):
-        over_z(n_out - 1)
+    for u in (n_out - 1, *range(max(n_out - 2, 0), n_out - 1)):
+        with jax.named_scope("over_z_last"):
+            over_z(u)
+    def result(u):
+        cut = pl.ds(u * LANES, LANES)
+        return pltpu.make_async_copy(done.at[u], out.at[:, cut], load_sem.at[u])
+
     with jax.named_scope("final"):
         for u in range(n_out):
             cut = slice(u * LANES, (u + 1) * LANES)
@@ -836,9 +879,16 @@
                 x_copy(u, MINE, dx).wait_recv()
             value = res[k, mine, cut].astype(jnp.float32) + place_sum(u, MINE)
             back(u).wait_recv()
-            out[:, cut] = (value + got_z[u].astype(jnp.float32)).astype(jnp.bfloat16)
+            value = value + got_z[u].astype(jnp.float32)
+            for dx in range(1, n_x) if u == n_out - 1 else ():
+                x_copy(u, THEIRS, dx).wait_recv()
+                value = value + got_x[u, THEIRS, dx - 1].astype(jnp.float32)
+            done[u] = value.astype(jnp.bfloat16)
+            result(u).start()
 
     with jax.named_scope("drain"):
+        for u in range(n_out):
+            result(u).wait()
         def drain(role):
             for i, view in enumerate(all_sums(role, n_from)):
                 to_y(view, view, y_send.at[i], y_recv.at[0]).wait_send()
@@ -889,7 +939,7 @@
             pl.BlockSpec(memory_space=pltpu.VMEM if i in in_vmem else pl.ANY)
             for i in range(len(args))
         ],
-        out_specs=pl.BlockSpec(memory_space=pltpu.VMEM),
+        out_specs=pl.BlockSpec(memory_space=pl.ANY),
         scratch_shapes=[
             held(width, 3 * (chans // 2)),
             held(n_fs, chans // 2, shard),
@@ -909,6 +959,7 @@
             held(n_out, 2, n_x, rows, LANES),
             held(n_out, 2, n_x - 1, rows, LANES),
             held(n_out, 2, n_x - 1, rows, LANES),
+            held(n_out, rows, LANES),
             held(n_out, rows, LANES),
             held(n_out, rows, LANES),
             dma((4, n_fs - 1)),

time: 136 us -> 133 us (0.978)
  Pallas kernels: 134 us -> 131 us
    pallas_call x1, Pallas kernels: 134 us -> 131 us  [fused(): pl.pallas_call(functools.partial(layer_kernel, n_fs, n_tp), out_shape=jax...]
where the time goes in v4:
time: 133 us
  Pallas kernels  131 us (98%)
  local copies, waits for them, and re-layouts  1.77 us (1%)
    pallas_call x1, Pallas kernels, fused(): pl.pallas_call(functools.partial(layer_kernel, n_fs, n_tp), out_shape=jax...  131 us

profile of v4, /device:TPU:0, one launch (start us, length us, event | category | flops | bytes accessed | tf_op | source)
XLA Modules:
  0.0 132.9 jit_solution(11699499275934920996)
XLA Ops:
  0.0 131.1 %shard_map.127 = bf16[384,512]{1,0:T(8,128)(2,1)} custom-call(bf16[384,512]{1,0:T(8,128)(2,1)} %tokens.1, f32[1,2048]{1,0:T(1,128)} %bitcast.4, bf16[512,256]{1,0:T(8,128)(2,1)} %w_signal.1, bf16[512,256]{1,0:T(8,128)(2,1)} %w_outer_gate.1, bf16[512,256]{1,0:T(8,128)(2,1)} %w_inner_gate.1, f32[3,256]{1,0:T(4,128)} %mix_taps.1, bf16[256,512]{1,0:T(8,128)(2,1)} %w_mix_out.1, ...), custom_call_target="tpu_custom_call" | custom-call | tf_op jit(solution)/shard_map/pallas_call | solution.py:935
  131.1 1.8 %copy.15 = bf16[384,512]{1,0:T(8,128)(2,1)} copy(bf16[384,512]{1,0:T(8,128)(2,1)} %shard_map.127) | data formatting | bytes 786432

commit v5 on v4

--- a/solution.py
+++ b/solution.py
@@ -122,19 +122,24 @@
     n_fs,
     n_tp,
     tokens,
-    mix_gain,
+    mix_gain_given,
     w_signal,
     w_outer_gate,
     w_inner_gate,
-    mix_taps,
+    mix_taps_given,
     w_mix_out,
-    ffn_gain,
+    ffn_gain_given,
     w_gate,
     w_value,
+    up_taps_given,
+    up_bias_given,
+    w_down,
+    out,
+    mix_gain,
+    mix_taps,
+    ffn_gain,
     up_taps,
     up_bias,
-    w_down,
-    out,
     mix_in,
     mix_out,
     ffn_in,
@@ -281,23 +286,27 @@
         copies = []
         for i, (src, dst) in enumerate(pairs):
             wide = i // 3 if s[0] == "mix" else 0
-            sems = z_send.at[group(s, wide), d - 1], z_recv.at[slot(s, wide), j]
+            sems = z_send.at[group(s, wide), d - 1], z_sem(s, wide, j, to)
             copies.append(to_fs(src, dst, *sems, to))
         return copies
 
     def z_takes(s, role, d):
         source = other(d)
         return [
-            to_fs(view, view, z_send.at[group(s, i), 0], z_recv.at[slot(s, i), source], source)
+            to_fs(view, view, z_send.at[group(s, i), 0], z_sem(s, i, source, j), source)
             for i, view in enumerate(places(s, role, source, g, True))
         ]
 
     def z_forwards(s):
         source = other(last)
+        to = other(1)
         return [
-            to_fs(view, view, f_send.at[group(s, i)], z_recv.at[slot(s, i), source], other(1))
+            to_fs(view, view, f_send.at[group(s, i)], z_sem(s, i, source, to), to)
             for i, view in enumerate(places(s, INNER, source, g, True))
         ]
+
+    def z_sem(s, i, source, to):
+        return z_recv.at[slot(s, i), lax.rem(source - to + n_fs, n_fs) - 1]
 
     def to_y(src, dst, send_sem, recv_sem):
         return pltpu.make_async_remote_copy(
@@ -309,9 +318,13 @@
             device_id_type=MESH,
         )
 
+    def late_d(role):
+        return 1 if role == INNER else 2
+
     def y_copies(s, role, d):
+        after = n_out if s[0] == "out" and d == late_d(role) else 0
         return [
-            to_y(view, view, y_send.at[group(s, i)], y_recv.at[slot(s, i)])
+            to_y(view, view, y_send.at[group(s, i)], y_recv.at[slot(s, i) + after])
             for i, view in enumerate(places(s, role, other(d), g, True))
         ]
 
@@ -372,6 +385,12 @@
     def arrived(s, role):
         for i, view in enumerate(sums(s, role, n_from)):
             to_y(view, view, y_send.at[group(s, i)], y_recv.at[slot(s, i)]).wait_recv()
+
+    def arrived_out(u, role, late):
+        s = outs[u]
+        (view,) = sums(s, role, 1 if late else n_from - 1)
+        at = slot(s, 0) + (n_out if late else 0)
+        to_y(view, view, y_send.at[group(s, 0)], y_recv.at[at]).wait_recv()
 
     def to_tp(src, dst, send_sem, recv_sem, to):
         return pltpu.make_async_remote_copy(
@@ -396,7 +415,7 @@
                 back = lax.rem(x + n_x - dx, n_x) * 2
                 seen = back + c if kind == "pass" else back + 1 - c
                 view = buffer.at[seen, at]
-                copies.append(to_tp(view, view, sent, all_recv.at[i, n_x - 1 + dx], core))
+                copies.append(to_tp(view, view, sent, all_recv.at[i, n_x - 1], core))
         return copies
 
     def all_begin(buffer, i, at):
@@ -412,7 +431,8 @@
             passed[dx].start()
 
     def all_end(buffer, i, at):
-        wait_recv(all_copies(buffer, i, at, "take"))
+        view = buffer.at[pl.ds(0, n_x), at]
+        to_tp(view, view, all_send.at[0], all_recv.at[i, n_x - 1], core).wait_recv()
 
     def to_pair(i, src, dst):
         return pltpu.make_async_remote_copy(
@@ -463,6 +483,20 @@
         pltpu.make_async_copy(src, dst, load_sem.at[i]).start()
 
     first.start()
+    small = [
+        pltpu.make_async_copy(src, dst, load_sem.at[5 + i])
+        for i, (src, dst) in enumerate(
+            (
+                (mix_gain_given, mix_gain),
+                (mix_taps_given, mix_taps),
+                (ffn_gain_given, ffn_gain),
+                (up_taps_given, up_taps),
+                (up_bias_given, up_bias),
+            )
+        )
+    ]
+    for copy in small:
+        copy.start()
     for i, ref in enumerate((w_signal, w_outer_gate, w_inner_gate)):
         load(0, ref.at[:, at_chans], mix_in.at[own_rows, pl.ds(i * unit_chans, unit_chans)])
     load(1, w_mix_out.at[at_chans, :], mix_out.at[j])
@@ -508,6 +542,8 @@
     by_role(begin)
     with jax.named_scope("loads"):
         by_role(wait_loads)
+        for copy in small:
+            copy.wait()
 
     def norm(buffer, at, gain):
         count = at.size
@@ -588,9 +624,13 @@
             part_mix.at[o, there * 2 + 1 - c],
             mix_core.at[o, there],
             mix_core_send.at[0],
-            mix_core_recv.at[o, dx],
+            mix_core_recv.at[o],
             core,
         )
+
+    def mix_core_wait(o):
+        view = part_mix.at[o, pl.ds(0, n_x)]
+        to_tp(view, mix_core.at[o], mix_core_send.at[0], mix_core_recv.at[o], core).wait_recv()
 
     def mix_x_copy(o, h, dx):
         to = lax.rem(x + dx, n_x) * 2 + c
@@ -629,12 +669,12 @@
 
     with jax.named_scope("mix_core"):
         for o in (THEIRS, MINE):
+            mix_core_wait(o)
             for dx in range(1, n_x):
-                mix_core_copy(o, dx).wait_recv()
                 for h in halves:
                     mix_x_sum[o, h, dx - 1] = mix_chip_sum(o, h, dx).astype(jnp.bfloat16)
                     mix_x_copy(o, h, dx).start()
-            mix_core_copy(o, 0).wait_recv()
+
     def between(role):
         if role == INNER:
             with jax.named_scope("ahead1"):
@@ -744,21 +784,17 @@
         unit = (gate / (1.0 + jnp.exp(-gate)) * value).astype(jnp.bfloat16)
         hidden[:, pl.ds(pl.multiple_of(t * LANES, LANES), LANES)] = unit
 
-    paced = {0: outs[:1], 2: outs[1:2], 3: outs[2:3]}
+    paced = {0: outs[:1], 2: outs[1:2], 3: outs[2:]}
     beside = {
         (INNER, 2): [(ins[5], 1), (ins[5], 2)],
-        (INNER, 3): [(outs[2], last), (outs[3], last)],
-        (INNER, 4): [(outs[0], 2), (outs[0], 1)],
+        (INNER, 4): [(outs[0], 2), (outs[2], last), (outs[3], last)],
+        (INNER, 5): [(outs[1], 2)],
         (END, 1): [(stage, 1) for stage in outs],
-        (END, 3): [(outs[0], last), (outs[0], 2)],
+        (END, 3): [(outs[0], last)],
     }
-    after = {
-        (INNER, 0): [(outs[1], 2), (outs[1], 1)],
-        (INNER, 1): [(outs[2], 2), (outs[2], 1)],
-        (INNER, 2): [(outs[3], 2), (outs[3], 1)],
-        (END, 0): [(outs[1], last), (outs[1], 2)],
-        (END, 1): [(outs[2], last), (outs[2], 2)],
-        (END, 2): [(outs[3], last), (outs[3], 2)],
+    ready = {
+        INNER: [[], [(outs[2], 2)], [(outs[3], 2)]],
+        END: [[(stage, last)] for stage in outs[1:]],
     }
 
     @pl.loop(0, jnp.where(at_end, tiles[END], tiles[INNER]))
@@ -781,10 +817,12 @@
 
         feed(t)
 
-    @pl.when(at_end)
-    def _():
-        for stage in outs[3:]:
-            send(stage, END, (2, last))
+    middle = n_fs // 2
+    left = j < middle
+    late_block = jnp.where(left, middle, middle - 1)
+
+    def when_block(block, late):
+        return pl.when(block == late_block if late else block != late_block)
 
     def core_copy(u, o, dx):
         there = lax.rem(x + dx, n_x)
@@ -819,54 +857,105 @@
             value = value + got_x[u, o, dx - 1].astype(jnp.float32)
         return value
 
-    def down(u, role):
-        with jax.named_scope("out_wait"):
-            arrived(("out", u), role)
-        deep = pl.ds(0, tiles[role] * LANES)
-        for o, at in ((THEIRS, theirs), (MINE, mine)):
-            left, right = hidden[at, deep], ffn_out[u, deep, :]
-            terms = jnp.dot(left, right, preferred_element_type=jnp.float32)
-            for b in range(n_tp):
-                part_ffn[u, o, b] = terms[:, b * LANES : (b + 1) * LANES].astype(jnp.bfloat16)
+    def product(u, o, deep, first, count):
+        at = theirs if o == THEIRS else mine
+        lanes = pl.ds(pl.multiple_of(first * LANES, LANES), count * LANES)
+        left_side, right_side = hidden[at, deep], ffn_out[u, deep, lanes]
+        terms = jnp.dot(left_side, right_side, preferred_element_type=jnp.float32)
+        for b in range(count):
+            part_ffn[u, o, first + b] = terms[:, b * LANES : (b + 1) * LANES].astype(jnp.bfloat16)
+
+    def down(u, late):
+        def body(role):
+            arrived_out(u, role, late)
+            deep = pl.ds(0, tiles[role] * LANES)
+            for o in (THEIRS, MINE):
+                if late:
+                    product(u, o, deep, late_block, 1)
+                else:
+                    product(u, o, deep, jnp.where(left, 0, middle), middle)
+                    product(u, o, deep, jnp.where(left, n_fs - 1, 0), 1)
+
+        with jax.named_scope("down_late" if late else "down"):
+            by_role(body)
+        for o in (THEIRS, MINE):
             for dx in (*range(1, n_x), 0):
-                core_copy(u, o, dx).start()
-
-    def over_x(u):
-        for o in (THEIRS, MINE):
-            for dx in range(1, n_x):
-                core_copy(u, o, dx).wait_recv()
-                sum_x[u, o, dx - 1] = chip_sum(u, o, dx).astype(jnp.bfloat16)
-                x_copy(u, o, dx).start()
-
-    def over_z(u):
-        core_copy(u, THEIRS, 0).wait_recv()
-        if u == n_out - 1:
-            value = chip_sum(u, THEIRS, 0)
-        else:
-            for dx in range(1, n_x):
-                x_copy(u, THEIRS, dx).wait_recv()
-            value = place_sum(u, THEIRS)
-        sum_z[u] = value.astype(jnp.bfloat16)
-        back(u).start()
-
-    for u in range(n_out):
-        if u >= 2:
+                block = lax.rem(x + dx, n_x) * 2 + 1 - c
+
+                @when_block(block, late)
+                def _():
+                    core_copy(u, o, dx).start()
+
+    def over_x(u, late):
+        for dx in range(1, n_x):
+
+            @when_block(lax.rem(x + dx, n_x) * 2 + c, late)
+            def _():
+                with jax.named_scope("over_x"):
+                    for o in (THEIRS, MINE):
+                        core_copy(u, o, dx).wait_recv()
+                        sum_x[u, o, dx - 1] = chip_sum(u, o, dx).astype(jnp.bfloat16)
+                        x_copy(u, o, dx).start()
+
+    def over_z(u, late):
+        @when_block(k, late)
+        def _():
             with jax.named_scope("over_z"):
-                over_z(u - 2)
-
-        def step(role):
-            for stage, d in after.get((role, u), ()):
-                with jax.named_scope("relay_out"):
+                core_copy(u, THEIRS, 0).wait_recv()
+                if u == n_out - 1:
+                    value = chip_sum(u, THEIRS, 0)
+                else:
+                    for dx in range(1, n_x):
+                        x_copy(u, THEIRS, dx).wait_recv()
+                    value = place_sum(u, THEIRS)
+                sum_z[u] = value.astype(jnp.bfloat16)
+                back(u).start()
+
+    def relay_late(u):
+        with jax.named_scope("relay_late"):
+            by_role(lambda role: relay(outs[u], role, late_d(role)))
+
+    def relay_ready(i):
+        def body(role):
+            for stage, d in ready[role][i]:
+                with jax.named_scope("relay_ready"):
                     relay(stage, role, d)
-            with jax.named_scope("down"):
-                down(u, role)
-
-        by_role(step)
-        with jax.named_scope("over_x"):
-            over_x(u)
-    for u in (n_out - 1, *range(max(n_out - 2, 0), n_out - 1)):
-        with jax.named_scope("over_z_last"):
-            over_z(u)
+
+        by_role(body)
+
+    early, late = False, True
+    relay_ready(0)
+    down(0, early)
+    relay_ready(1)
+    over_x(0, early)
+    down(1, early)
+    relay_ready(2)
+    relay_late(0)
+    over_x(1, early)
+    down(2, early)
+    over_x(2, early)
+    down(3, early)
+    relay_late(1)
+    over_x(3, early)
+    over_z(3, early)
+    down(0, late)
+    relay_late(2)
+    over_x(0, late)
+    over_z(0, early)
+    down(1, late)
+    relay_late(3)
+    over_x(1, late)
+    over_z(1, early)
+    down(2, late)
+    over_x(2, late)
+    over_z(0, late)
+    down(3, late)
+    over_x(3, late)
+    over_z(3, late)
+    over_z(2, early)
+    over_z(1, late)
+    over_z(2, late)
+
     def result(u):
         cut = pl.ds(u * LANES, LANES)
         return pltpu.make_async_copy(done.at[u], out.at[:, cut], load_sem.at[u])
@@ -924,7 +1013,7 @@
     args = list(args)
     args[1], args[7] = args[1].reshape(1, -1), args[7].reshape(1, -1)
     args[10] = args[10].transpose(1, 0, 2)
-    in_vmem = {1, 5, 7, 10, 11}
+    small = [pltpu.VMEM(args[i].shape, jnp.float32) for i in (1, 5, 7, 10, 11)]
     n_x = n_tp // 2
     length = rows // SEQS_DEV
     dma = pltpu.SemaphoreType.DMA
@@ -935,12 +1024,10 @@
     return pl.pallas_call(
         functools.partial(layer_kernel, n_fs, n_tp),
         out_shape=jax.ShapeDtypeStruct((rows, cols), jnp.bfloat16),
-        in_specs=[
-            pl.BlockSpec(memory_space=pltpu.VMEM if i in in_vmem else pl.ANY)
-            for i in range(len(args))
-        ],
+        in_specs=[pl.BlockSpec(memory_space=pl.ANY)] * len(args),
         out_specs=pl.BlockSpec(memory_space=pl.ANY),
         scratch_shapes=[
+            *small,
             held(width, 3 * (chans // 2)),
             held(n_fs, chans // 2, shard),
             held(n_in, width, 2 * LANES),
@@ -963,15 +1050,15 @@
             held(n_out, rows, LANES),
             held(n_out, rows, LANES),
             dma((4, n_fs - 1)),
-            dma((2 + n_in + n_out, n_fs)),
+            dma((2 + n_in + n_out, n_fs - 1)),
             dma((4,)),
             dma((4,)),
-            dma((2 + n_in + n_out,)),
-            dma((5,)),
+            dma((2 + n_in + 2 * n_out,)),
+            dma((10,)),
             dma((2,)),
-            dma((1 + 3 * SEQS_DEV, 2 * n_x - 1)),
+            dma((1 + 3 * SEQS_DEV, n_x)),
             dma((1,)),
-            dma((2, n_x)),
+            dma((2,)),
             dma((1,)),
             dma((2, SEQS_DEV, n_x - 1)),
             dma((1,)),

time: 133 us -> 129 us (0.970)
  Pallas kernels: 131 us -> 127 us
    pallas_call x1, Pallas kernels: 131 us -> 127 us  [fused(): pl.pallas_call(functools.partial(layer_kernel, n_fs, n_tp), out_shape=jax...]
where the time goes in v5:
time: 129 us
  Pallas kernels  127 us (98%)
  local copies, waits for them, and re-layouts  1.77 us (1%)
    pallas_call x1, Pallas kernels, fused(): pl.pallas_call(functools.partial(layer_kernel, n_fs, n_tp), out_shape=jax...  127 us

profile of v5, /device:TPU:0, one launch (start us, length us, event | category | flops | bytes accessed | tf_op | source)
XLA Modules:
  0.0 128.7 jit_solution(17552584919922599937)
XLA Ops:
  0.0 126.9 %shard_map.127 = bf16[384,512]{1,0:T(8,128)(2,1)} custom-call(bf16[384,512]{1,0:T(8,128)(2,1)} %tokens.1, f32[1,2048]{1,0:T(1,128)} %bitcast.4, bf16[512,256]{1,0:T(8,128)(2,1)} %w_signal.1, bf16[512,256]{1,0:T(8,128)(2,1)} %w_outer_gate.1, bf16[512,256]{1,0:T(8,128)(2,1)} %w_inner_gate.1, f32[3,256]{1,0:T(4,128)} %mix_taps_given.1, ...), custom_call_target="tpu_custom_call" | custom-call | tf_op jit(solution)/shard_map/pallas_call | solution.py:1024
  127.0 1.8 %copy.15 = bf16[384,512]{1,0:T(8,128)(2,1)} copy(bf16[384,512]{1,0:T(8,128)(2,1)} %shard_map.127) | data formatting | bytes 786432

commit v6 on v5

--- a/solution.py
+++ b/solution.py
@@ -787,13 +787,13 @@
     paced = {0: outs[:1], 2: outs[1:2], 3: outs[2:]}
     beside = {
         (INNER, 2): [(ins[5], 1), (ins[5], 2)],
-        (INNER, 4): [(outs[0], 2), (outs[2], last), (outs[3], last)],
+        (INNER, 4): [(outs[0], 2)],
         (INNER, 5): [(outs[1], 2)],
         (END, 1): [(stage, 1) for stage in outs],
         (END, 3): [(outs[0], last)],
     }
     ready = {
-        INNER: [[], [(outs[2], 2)], [(outs[3], 2)]],
+        INNER: [[(outs[2], last)], [(outs[2], 2)], [(outs[3], last), (outs[3], 2)]],
         END: [[(stage, last)] for stage in outs[1:]],
     }
 
@@ -933,26 +933,26 @@
     relay_late(0)
     over_x(1, early)
     down(2, early)
+    relay_late(1)
     over_x(2, early)
     down(3, early)
-    relay_late(1)
     over_x(3, early)
     over_z(3, early)
+    relay_late(2)
     down(0, late)
-    relay_late(2)
     over_x(0, late)
     over_z(0, early)
     down(1, late)
+    over_x(1, late)
     relay_late(3)
-    over_x(1, late)
     over_z(1, early)
     down(2, late)
     over_x(2, late)
     over_z(0, late)
+    over_z(2, early)
     down(3, late)
     over_x(3, late)
     over_z(3, late)
-    over_z(2, early)
     over_z(1, late)
     over_z(2, late)
 

time: 129 us -> 128 us (level)
  Pallas kernels: 127 us -> 125 us
    pallas_call x1, Pallas kernels: 127 us -> 125 us  [fused(): pl.pallas_call(functools.partial(layer_kernel, n_fs, n_tp), out_shape=jax...]
where the time goes in v6:
time: 128 us; the launch traced here: 126 us
  Pallas kernels  125 us (98%)
  local copies, waits for them, and re-layouts  1.77 us (1%)
    pallas_call x1, Pallas kernels, fused(): pl.pallas_call(functools.partial(layer_kernel, n_fs, n_tp), out_shape=jax...  125 us

profile of v6, /device:TPU:0, one launch (start us, length us, event | category | flops | bytes accessed | tf_op | source)
XLA Modules:
  0.0 126.5 jit_solution(13535177038144945097)
XLA Ops:
  0.0 124.7 %shard_map.127 = bf16[384,512]{1,0:T(8,128)(2,1)} custom-call(bf16[384,512]{1,0:T(8,128)(2,1)} %tokens.1, f32[1,2048]{1,0:T(1,128)} %bitcast.4, bf16[512,256]{1,0:T(8,128)(2,1)} %w_signal.1, bf16[512,256]{1,0:T(8,128)(2,1)} %w_outer_gate.1, bf16[512,256]{1,0:T(8,128)(2,1)} %w_inner_gate.1, f32[3,256]{1,0:T(4,128)} %mix_taps_given.1, ...), custom_call_target="tpu_custom_call" | custom-call | tf_op jit(solution)/shard_map/pallas_call | solution.py:1024
  124.7 1.8 %copy.15 = bf16[384,512]{1,0:T(8,128)(2,1)} copy(bf16[384,512]{1,0:T(8,128)(2,1)} %shard_map.127) | data formatting | bytes 786432

commit v7 on v6

--- a/solution.py
+++ b/solution.py
@@ -784,7 +784,7 @@
         unit = (gate / (1.0 + jnp.exp(-gate)) * value).astype(jnp.bfloat16)
         hidden[:, pl.ds(pl.multiple_of(t * LANES, LANES), LANES)] = unit
 
-    paced = {0: outs[:1], 2: outs[1:2], 3: outs[2:]}
+    paced = {1: outs[:1], 2: outs[1:2], 3: outs[2:]}
     beside = {
         (INNER, 2): [(ins[5], 1), (ins[5], 2)],
         (INNER, 4): [(outs[0], 2)],
@@ -950,10 +950,10 @@
     over_x(2, late)
     over_z(0, late)
     over_z(2, early)
+    over_z(1, late)
     down(3, late)
     over_x(3, late)
     over_z(3, late)
-    over_z(1, late)
     over_z(2, late)
 
     def result(u):

time: 128 us -> 128 us (level)
  no operation moved by 1% of the time
where the time goes in v7:
time: 128 us; the launch traced here: 127 us
  Pallas kernels  125 us (98%)
  local copies, waits for them, and re-layouts  1.77 us (1%)
    pallas_call x1, Pallas kernels, fused(): pl.pallas_call(functools.partial(layer_kernel, n_fs, n_tp), out_shape=jax...  125 us

profile of v7, /device:TPU:0, one launch (start us, length us, event | category | flops | bytes accessed | tf_op | source)
XLA Modules:
  0.0 126.6 jit_solution(9946903830933936756)
XLA Ops:
  0.0 124.9 %shard_map.127 = bf16[384,512]{1,0:T(8,128)(2,1)} custom-call(bf16[384,512]{1,0:T(8,128)(2,1)} %tokens.1, f32[1,2048]{1,0:T(1,128)} %bitcast.4, bf16[512,256]{1,0:T(8,128)(2,1)} %w_signal.1, bf16[512,256]{1,0:T(8,128)(2,1)} %w_outer_gate.1, bf16[512,256]{1,0:T(8,128)(2,1)} %w_inner_gate.1, f32[3,256]{1,0:T(4,128)} %mix_taps_given.1, ...), custom_call_target="tpu_custom_call" | custom-call | tf_op jit(solution)/shard_map/pallas_call | solution.py:1024
  124.9 1.8 %copy.15 = bf16[384,512]{1,0:T(8,128)(2,1)} copy(bf16[384,512]{1,0:T(8,128)(2,1)} %shard_map.127) | data formatting | bytes 786432
